TPU v7x, 512 devices: a whole 4x4x16 slice. The times are simulated.
512 devices in a mesh: ep: 128 (over z, x, core), tp: 4 (over y).
Axes of the slice: x: 4, y: 4, z: 16, core: 2. Of those that a mesh axis runs over, the one named last changes fastest.
Arguments:
- tokens: bfloat16 [3072, 2048], P('ep'), may hold values from -24 to 24
- carried_state: float32 [3072, 4, 128, 128], P('ep', 'tp'), may hold values from -4 to 4
- w_query: bfloat16 [2048, 512], P(None, 'tp'), may hold values from -0.125 to 0.125
- w_forget: bfloat16 [2048, 512], P(None, 'tp'), may hold values from -0.125 to 0.125
- w_value: bfloat16 [2048, 512], P(None, 'tp'), may hold values from -0.125 to 0.125
- forget_floor: float32 [4, 128], P('tp'), may hold values from 0.05 to 0.9
- head_gain: bfloat16 [4, 128], P('tp'), may hold values from 0.099609375 to 1.8984375
- w_out: bfloat16 [512, 2048], P('tp', 'ep'), may hold values from -0.25 to 0.25
- gain_mix: bfloat16 [2048], replicated, may hold values from 0.099609375 to 1.8984375
- gain_ffn: bfloat16 [2048], replicated, may hold values from 0.099609375 to 1.8984375
- gain_post: bfloat16 [2048], P('tp'), may hold values from 0.099609375 to 1.8984375
- w_branch_gate: bfloat16 [2048], replicated, may hold values from -0.125 to 0.125
- shared_gate: bfloat16 [2048, 512], P('ep', 'tp'), may hold values from -0.125 to 0.125
- shared_up: bfloat16 [2048, 512], P('ep', 'tp'), may hold values from -0.125 to 0.125
- shared_down: bfloat16 [512, 2048], P('tp', 'ep'), may hold values from -1.1048543 to 1.1048543
- routes: int32 [3072, 6], P('ep'), may hold values from 0 to 127, all different within a row; in each aligned block of 24 rows (0 to 23, 24 to 47, ...) at most 2 rows name the same one
- route_weights: float32 [3072, 6], P('ep'), may hold values from 0.2 to 1
- expert_gate: bfloat16 [128, 2048, 512], P('ep', None, 'tp'), may hold values from -0.125 to 0.125
- expert_up: bfloat16 [128, 2048, 512], P('ep', None, 'tp'), may hold values from -0.125 to 0.125
- expert_down: bfloat16 [128, 512, 2048], P('ep', 'tp'), may hold values from -1.1048543 to 1.1048543
Outputs:
- layer_out: bfloat16 [3072, 2048], P('ep', 'tp')
- new_state: float32 [3072, 4, 128, 128], P('ep', 'tp')
Inputs may be any that keep to these rules, and one draw needn't show every extreme that they name: `routes`: among the 24 rows of one index of ep, no expert is named by more than 2 rows, a bound that some block reaches.
All inputs are finite; a program needn't handle non-finite values.
Results may differ from a plain program's by a relative error of at most 0.015.
Values may be sent and summed in bfloat16 or wider, within the bound.
No kernel may reach another device: no remote copies, remote signals or barrier semaphores. Data moves between devices by JAX's collectives and lax.ppermute only.
A program may use at most 64 MiB of HBM per device.

v0:
```python
import jax
import jax.numpy as jnp
from jax import lax
from jax.experimental import pallas as pl
from jax.experimental.pallas import tpu as pltpu
from jax.sharding import Mesh
from jax.sharding import PartitionSpec as P

EP = ("ep_0", "ep_1", "ep_2")
epsilon = 1e-06
BF = jnp.bfloat16
F32 = jnp.float32
NT = (((1,), (1,)), ((), ()))


def exchanged(value, axes):
    return lax.all_to_all(value, axes, 0, 0, tiled=True)


def to_all(value, axes):
    devices = lax.axis_size(axes)
    return exchanged(jnp.broadcast_to(value[None], (devices, *value.shape)), axes)


def rmsnorm(values_in, gain):
    scale = lax.rsqrt(jnp.mean(values_in * values_in, axis=-1, keepdims=True) + epsilon)
    return values_in * scale * gain.astype(F32)


def from_z_order(cores, zs, inverse):
    n = cores * zs * 2
    core_major = lax.broadcasted_iota(jnp.int32, (n, n), 1 if inverse else 0)
    z_major = lax.broadcasted_iota(jnp.int32, (n, n), 0 if inverse else 1)
    core, z, slot = core_major // (2 * zs), (core_major // 2) % zs, core_major % 2
    return jnp.where(z_major == (z * cores + core) * 2 + slot, 1.0, 0.0).astype(BF)


def vmem_call(body, out_shape, args, scratch=(), limit=32):
    vmem = pl.BlockSpec(memory_space=pltpu.VMEM)
    return pl.pallas_call(
        body,
        out_shape=out_shape,
        in_specs=[vmem] * len(args),
        out_specs=jax.tree.map(lambda _: vmem, out_shape),
        scratch_shapes=list(scratch),
        compiler_params=pltpu.CompilerParams(vmem_limit_bytes=limit * 1024 * 1024),
    )(*args)


def dispatch_body(terms, places, tok, chosen, resid, send):
    mixed = jnp.zeros(tok.shape, F32)
    for k in range(terms.shape[0]):
        part = terms[k, 0].astype(F32)
        for t in range(1, terms.shape[1]):
            part = part + terms[k, t].astype(F32)
        mixed = mixed + jnp.dot(part.astype(BF), places[k], preferred_element_type=F32)
    summed = (tok[...].astype(F32) + mixed).astype(BF)
    resid[...] = summed
    send[...] = jnp.dot(chosen[...], summed, preferred_element_type=F32).astype(BF)


def spread_body(arrived, out):
    cores, n_tp, rows, width = out.shape
    perm = from_z_order(cores, rows // 2, False)
    moved = jnp.dot(perm, arrived[...], preferred_element_type=F32).astype(BF)
    for t in range(n_tp):
        out[:, t] = moved.reshape(cores, rows, width)


def collect_body(terms, out):
    cores, n_tp, rows, width = terms.shape
    total = terms[:, 0].astype(F32)
    for t in range(1, n_tp):
        total = total + terms[:, t].astype(F32)
    perm = from_z_order(cores, rows // 2, True)
    total = total.astype(BF).reshape(cores * rows, width)
    out[...] = jnp.dot(perm, total, preferred_element_type=F32).astype(BF)


def normed_columns(x, gain, hn):
    slice_width = hn.shape[1] // x[0]
    squares = None
    for j in range(x[0]):
        wide = x[1](j).astype(F32)
        part = jnp.sum(wide * wide, axis=1, keepdims=True)
        squares = part if squares is None else squares + part
    scale = lax.rsqrt(squares / hn.shape[1] + epsilon)
    for j in range(x[0]):
        cols = pl.ds(j * slice_width, slice_width)
        hn[:, cols] = (x[1](j).astype(F32) * scale * gain[:, cols].astype(F32)).astype(BF)


def expert_body(x, gain, gate_hbm, up_hbm, down_hbm, out, hn, gate_w, up_w, down_w, sems):
    cores, n_tp, rows, slice_width = x.shape
    total = cores * rows
    copies = [
        pltpu.make_async_copy(src, dst, sems.at[k])
        for k, (src, dst) in enumerate(
            ((gate_hbm, gate_w), (up_hbm, up_w), (down_hbm, down_w))
        )
    ]
    for copy in copies:
        copy.start()
    normed_columns((n_tp, lambda j: x[:, j].reshape(total, slice_width)), gain, hn)
    copies[0].wait()
    gate_pre = jnp.dot(hn[...], gate_w[...], preferred_element_type=F32)
    copies[1].wait()
    up_pre = jnp.dot(hn[...], up_w[...], preferred_element_type=F32)
    hidden = (gate_pre * jax.nn.sigmoid(gate_pre) * up_pre).astype(BF)
    copies[2].wait()
    for j in range(n_tp):
        cols = pl.ds(j * slice_width, slice_width)
        part = jnp.dot(hidden, down_w[:, cols], preferred_element_type=F32).astype(BF)
        out[:, j] = part.reshape(cores, rows, slice_width)


def expert_kernel(x, gain, gate_w, up_w, down_w):
    cores, n_tp, rows, slice_width = x.shape
    vmem = pl.BlockSpec(memory_space=pltpu.VMEM)
    hbm = pl.BlockSpec(memory_space=pl.ANY)
    return pl.pallas_call(
        expert_body,
        out_shape=jax.ShapeDtypeStruct(x.shape, BF),
        in_specs=[vmem, vmem, hbm, hbm, hbm],
        out_specs=vmem,
        scratch_shapes=[
            pltpu.VMEM((cores * rows, n_tp * slice_width), BF),
            pltpu.VMEM(gate_w.shape, BF),
            pltpu.VMEM(up_w.shape, BF),
            pltpu.VMEM(down_w.shape, BF),
            pltpu.SemaphoreType.DMA((3,)),
        ],
        compiler_params=pltpu.CompilerParams(vmem_limit_bytes=32 * 1024 * 1024),
        name="expert",
    )(x, gain, gate_w, up_w, down_w)


def shared_body(x, gain, mix_w, gate_w, up_w, down_w, out, mix, hn):
    n_tp = x.shape[0]
    normed_columns((n_tp, lambda j: x[j]), gain, hn)
    logits = jnp.sum(hn[...].astype(F32) * mix_w[...].astype(F32), axis=1, keepdims=True)
    mix[...] = jnp.broadcast_to(jax.nn.sigmoid(logits), mix.shape)
    gate_pre = jnp.dot(hn[...], gate_w[...], preferred_element_type=F32)
    up_pre = jnp.dot(hn[...], up_w[...], preferred_element_type=F32)
    hidden = (gate_pre * jax.nn.sigmoid(gate_pre) * up_pre).astype(BF)
    out[...] = lax.dot_general(hidden, down_w[...], NT, preferred_element_type=F32).astype(BF)


def shards(
    tokens,
    carried_state,
    w_query,
    w_forget,
    w_value,
    forget_floor,
    head_gain,
    w_out,
    gain_mix,
    gain_ffn,
    gain_post,
    w_branch_gate,
    shared_gate,
    shared_up,
    shared_down,
    routes,
    route_weights,
    expert_gate,
    expert_up,
    expert_down,
):
    seq_rows, model_width = tokens.shape
    head_dim = carried_state.shape[2]
    n_ep = lax.axis_size(EP)
    n_z = lax.axis_size("ep_0")
    n_tp = lax.axis_size("tp")
    cores = n_ep // n_z
    piece = w_out.shape[1]
    slice_width = model_width // n_tp
    slots_all = 2 * n_ep
    here = lax.axis_index("tp")
    parts = to_all(jnp.stack([w_out.T, shared_gate, shared_up, shared_down.T]), "ep_0")
    column = lax.broadcasted_iota(jnp.int32, (1, 1, slots_all), 2)
    hits = routes[:, :, None] == column // 2
    named = jnp.any(hits, axis=1).astype(BF)
    tri = (
        lax.broadcasted_iota(jnp.int32, (seq_rows, seq_rows), 0)
        > lax.broadcasted_iota(jnp.int32, (seq_rows, seq_rows), 1)
    ).astype(BF)
    rank = jnp.dot(tri, named, preferred_element_type=F32)
    taken = (named > 0) & (rank == (column[0] % 2).astype(F32))
    chosen = jnp.where(taken, 1.0, 0.0).astype(BF).T
    combine = jnp.where(taken, jnp.sum(jnp.where(hits, route_weights[:, :, None], 0.0), axis=1), 0.0)
    normed = rmsnorm(tokens.astype(F32), gain_mix).astype(BF)
    queries = jax.nn.silu(jnp.dot(normed, w_query, preferred_element_type=F32))
    forget_pre = jnp.dot(normed, w_forget, preferred_element_type=F32)
    values_in = jnp.dot(normed, w_value, preferred_element_type=F32)
    queries = queries.reshape(seq_rows, 1, head_dim)
    forget_pre = forget_pre.reshape(seq_rows, 1, head_dim)
    values_in = values_in.reshape(seq_rows, 1, head_dim)
    forget = forget_floor + (1.0 - forget_floor) * jax.nn.sigmoid(forget_pre)
    keys_in = (1.0 - forget_floor) * jax.nn.sigmoid(-forget_pre)
    new_state = forget[..., None] * carried_state + keys_in[..., None] * values_in[:, :, None, :]
    readout = jnp.einsum("bhd,bhdv->bhv", queries, new_state, precision=lax.Precision.HIGHEST)
    head_out = rmsnorm(readout, head_gain).astype(BF).reshape(seq_rows, head_dim)
    heads = lax.all_gather(head_out, "ep_2")
    heads = lax.all_gather(heads, "ep_1").reshape(cores * seq_rows, head_dim)
    line_w = parts[:, 0].reshape(n_z * piece, head_dim)
    terms = lax.dot_general(heads, line_w, NT, preferred_element_type=F32).astype(BF)
    own = n_z * piece // n_tp
    per = 128 // own
    terms = terms.reshape(cores, 1, seq_rows, n_tp // per, 128)
    terms = jnp.broadcast_to(terms, (cores, per, seq_rows, n_tp // per, 128))
    terms = terms.transpose(0, 3, 1, 2, 4).reshape(cores * n_tp, seq_rows, 128)
    terms = exchanged(terms, ("ep_1", "ep_2", "tp"))
    terms = terms.reshape(cores, n_tp, seq_rows, 128)
    core = lax.broadcasted_iota(jnp.int32, (cores, 128, slice_width), 0)
    lane = lax.broadcasted_iota(jnp.int32, (cores, 128, slice_width), 1) - own * (here % per)
    target = lax.broadcasted_iota(jnp.int32, (cores, 128, slice_width), 2)
    places = (
        (lane >= 0)
        & (lane < own)
        & (target == (lane // piece * cores + core) * piece + lane % piece)
    )
    places = jnp.where(places, 1.0, 0.0).astype(BF)
    token_slice = lax.dynamic_slice_in_dim(tokens, here * slice_width, slice_width, 1)
    resid, send = vmem_call(
        dispatch_body,
        (
            jax.ShapeDtypeStruct((seq_rows, slice_width), BF),
            jax.ShapeDtypeStruct((slots_all, slice_width), BF),
        ),
        (terms, places, token_slice, chosen),
    )
    arrived = exchanged(send.reshape(n_z, 2 * cores, slice_width), "ep_0")
    mine = lax.all_gather(resid, "tp")
    spread = vmem_call(
        spread_body,
        jax.ShapeDtypeStruct((cores, n_tp, 2 * n_z, slice_width), BF),
        (arrived.reshape(slots_all, slice_width),),
    )
    plane = (cores * n_tp, 2 * n_z, slice_width)
    x = exchanged(spread.reshape(plane), ("ep_1", "ep_2", "tp")).reshape(spread.shape)
    down_terms = expert_kernel(x, gain_ffn[None], expert_gate[0], expert_up[0], expert_down[0])
    down_terms = exchanged(down_terms.reshape(plane), ("ep_1", "ep_2", "tp"))
    summed = vmem_call(
        collect_body,
        jax.ShapeDtypeStruct((slots_all, slice_width), BF),
        (down_terms.reshape(spread.shape),),
    )
    returned = exchanged(summed.reshape(n_z, 2 * cores, slice_width), "ep_0")
    returned = returned.reshape(slots_all, slice_width)
    shared = lax.all_gather(parts[:, 1:], "ep_1")
    other = lax.ppermute(shared, "ep_2", [(0, 1), (1, 0)])
    first = lax.axis_index("ep_2") == 0
    shared = jnp.stack([jnp.where(first, shared, other), jnp.where(first, other, shared)])
    shared = shared.transpose(3, 2, 1, 0, 4, 5).reshape(3, model_width, head_dim)
    shared_terms, mix = vmem_call(
        shared_body,
        (
            jax.ShapeDtypeStruct((seq_rows, model_width), BF),
            jax.ShapeDtypeStruct((seq_rows, 128), F32),
        ),
        (mine, gain_ffn[None], w_branch_gate[None], shared[0], shared[1], shared[2]),
        (pltpu.VMEM((seq_rows, model_width), BF),),
    )
    shared_terms = lax.all_gather(shared_terms, "tp")
    shared_terms = lax.dynamic_slice_in_dim(shared_terms, here * slice_width, slice_width, 2)
    shared_out = jnp.sum(shared_terms.astype(F32), axis=0).astype(BF)
    routed = jnp.dot(combine, returned.astype(F32), precision=lax.Precision.HIGHEST)
    branch_sum = routed + mix[:, :1] * shared_out.astype(F32)
    square_part = jnp.sum(branch_sum * branch_sum, axis=1)
    square_total = jnp.sum(to_all(square_part, "tp"), axis=0)
    norm_scale = lax.rsqrt(square_total / model_width + epsilon)
    layer_out = resid.astype(F32) + branch_sum * norm_scale[:, None] * gain_post.astype(F32)
    return (layer_out.astype(BF), new_state)


def solution(mesh):
    torus = Mesh(mesh.devices.reshape(16, 4, 2, mesh.shape["tp"]), ("ep_0", "ep_1", "ep_2", "tp"))
    in_specs = (
        P(EP, None),
        P(EP, "tp", None, None),
        P(None, "tp"),
        P(None, "tp"),
        P(None, "tp"),
        P("tp", None),
        P("tp", None),
        P("tp", EP),
        P(),
        P(),
        P("tp"),
        P(),
        P(EP, "tp"),
        P(EP, "tp"),
        P("tp", EP),
        P(EP, None),
        P(EP, None),
        P(EP, None, "tp"),
        P(EP, None, "tp"),
        P(EP, "tp", None),
    )
    out_specs = (P(EP, "tp"), P(EP, "tp", None, None))

    return jax.shard_map(
        shards, mesh=torus, in_specs=in_specs, out_specs=out_specs, check_vma=False
    )
```

profile of v0, /device:TPU:32, one launch (start us, length us, event | category | flops | bytes accessed | tf_op | source)
XLA Modules:
  0.0 191.2 jit_solution(10191428871067467379)
XLA Ops:
  0.7 0.9 pad_maximum_fusion
  1.6 0.8 broadcast_in_dim.42
  2.3 15.2 %all-to-all-start = ((bf16[16,4,16,128]{3,2,1,0:T(8,128)(2,1)}), bf16[16,4,16,128]{3,2,1,0:T(8,128)(2,1)S(1)}, u32[]{:S(2)}, u32[]{:S(2)}) async-start(bf16[16,4,16,128]{3,2,1,0:T(8,128)(2,1)} %broadcast_in_dim.42), calls=%async_computation | async-start | bytes 524288 | tf_op jit(solution)/shard_map/all_to_all | solution.py:17
  17.6 0.7 bitcast_convert_fusion
  18.9 1.0 fusion.4
  19.9 0.7 convert_element_type.52
  20.6 1.3 fusion.15
  22.5 1.0 multiply_add_fusion
  23.6 1.1 copy-done.4
  24.7 1.4 fusion.1
  26.6 1.8 all-gather
  28.4 12.3 %all-gather.1 = bf16[8,24,128]{2,1,0:T(8,128)(2,1)S(1)} all-gather(bf16[2,24,128]{2,1,0:T(8,128)(2,1)S(1)} %bitcast.84), channel_id=3, replica_groups=mesh['ep_0'=16,'ep_1'=4,'ep_2'=2,'tp'=4] {'ep_1'}, dimensions={0}, use_global_device_ids=true | all-gather | bytes 61440 | tf_op jit(solution)/shard_map/all_gather | solution.py:206
  40.9 0.7 select_convert_fusion.places
  41.9 0.7 broadcast_in_dim.44
  42.6 6.7 %all-to-all-start.1 = ((bf16[32,24,128]{2,1,0:T(8,128)(2,1)}), bf16[32,24,128]{2,1,0:T(8,128)(2,1)S(1)}, u32[]{:S(2)}, u32[]{:S(2)}) async-start(bf16[32,24,128]{2,1,0:T(8,128)(2,1)} %bitcast.18), calls=%async_computation.1 | async-start | bytes 393216 | tf_op jit(solution)/shard_map/all_to_all | solution.py:17
  49.4 8.4 %all-to-all-done.1 = bf16[32,24,128]{2,1,0:T(8,128)(2,1)S(1)} async-done(((bf16[32,24,128]{2,1,0:T(8,128)(2,1)}), bf16[32,24,128]{2,1,0:T(8,128)(2,1)S(1)}, u32[]{:S(2)}, u32[]{:S(2)}) %all-to-all-start.1) | async-done | bytes 196640 | tf_op jit(solution)/shard_map/all_to_all | solution.py:17
  58.3 30.0 %all_to_all.36 = bf16[16,16,512]{2,1,0:T(8,128)(2,1)S(1)} all-to-all(bf16[16,16,512]{2,1,0:T(8,128)(2,1)S(1)} %bitcast.74), channel_id=1, replica_groups=mesh['ep_0'=16,'ep_1'=4,'ep_2'=2,'tp'=4] {'ep_0'}, dimensions={0} | all-to-all | bytes 524288 | tf_op jit(solution)/shard_map/all_to_all | solution.py:17
  88.3 1.2 shard_map.204
  89.6 4.1 %all-to-all-start.3 = ((bf16[32,32,512]{2,1,0:T(8,128)(2,1)}), bf16[32,32,512]{2,1,0:T(8,128)(2,1)S(1)}, u32[]{:S(2)}, u32[]{:S(2)}) async-start(bf16[32,32,512]{2,1,0:T(8,128)(2,1)} %bitcast.23), calls=%async_computation.3 | async-start | bytes 2097152 | tf_op jit(solution)/shard_map/all_to_all | solution.py:17
  93.7 17.0 %all-to-all-done.3 = bf16[32,32,512]{2,1,0:T(8,128)(2,1)S(1)} async-done(((bf16[32,32,512]{2,1,0:T(8,128)(2,1)}), bf16[32,32,512]{2,1,0:T(8,128)(2,1)S(1)}, u32[]{:S(2)}, u32[]{:S(2)}) %all-to-all-start.3) | async-done | bytes 1048608 | tf_op jit(solution)/shard_map/all_to_all | solution.py:17
  110.7 2.9 %expert.1 = bf16[8,4,32,512]{3,2,1,0:T(8,128)(2,1)} custom-call(bf16[8,4,32,512]{3,2,1,0:T(8,128)(2,1)S(1)} %bitcast.63, bf16[1,2048]{1,0:T(2,128)(2,1)S(1)} %broadcast_in_dim.78.gain, bf16[2048,128]{1,0:T(8,128)(2,1)S(1)} %bitcast.70, bf16[2048,128]{1,0:T(8,128)(2,1)S(1)} %bitcast.71, bf16[128,2048]{1,0:T(8,128)(2,1)S(1)} %bitcast.72), custom_call_target="tpu_custom_call" | custom-call | tf_op jit(solution)/shard_map/expert/pallas_call | solution.py:121
  113.6 4.1 %all-to-all-start.4 = ((bf16[32,32,512]{2,1,0:T(8,128)(2,1)}), bf16[32,32,512]{2,1,0:T(8,128)(2,1)S(1)}, u32[]{:S(2)}, u32[]{:S(2)}) async-start(bf16[32,32,512]{2,1,0:T(8,128)(2,1)} %bitcast.28), calls=%async_computation.4 | async-start | bytes 2097152 | tf_op jit(solution)/shard_map/all_to_all | solution.py:17
  117.7 24.9 %all-gather.3 = bf16[64,3,16,128]{3,2,1,0:T(8,128)(2,1)S(1)} all-gather(bf16[16,3,16,128]{3,2,1,0:T(8,128)(2,1)S(1)} %slice-done), channel_id=5, replica_groups=mesh['ep_0'=16,'ep_1'=4,'ep_2'=2,'tp'=4] {'ep_1'}, dimensions={0}, use_global_device_ids=true | all-gather | bytes 983040 | tf_op jit(solution)/shard_map/all_gather | solution.py:252
  142.6 1.9 collective-permute-start
  144.7 12.2 %all-gather.2 = bf16[96,512]{1,0:T(8,128)(2,1)S(1)} all-gather(bf16[24,512]{1,0:T(8,128)(2,1)S(1)} %get-tuple-element.6), channel_id=4, replica_groups=mesh['ep_0'=16,'ep_1'=4,'ep_2'=2,'tp'=4] {'tp'}, dimensions={0}, use_global_device_ids=true | all-gather | bytes 122880 | tf_op jit(solution)/shard_map/all_gather | solution.py:235
  157.0 1.0 shard_map.205
  158.0 6.1 %all-to-all-start.5 = ((bf16[16,16,512]{2,1,0:T(8,128)(2,1)}), bf16[16,16,512]{2,1,0:T(8,128)(2,1)S(1)}, u32[]{:S(2)}, u32[]{:S(2)}) async-start(bf16[16,16,512]{2,1,0:T(8,128)(2,1)} %bitcast.30), calls=%async_computation.5 | async-start | bytes 524288 | tf_op jit(solution)/shard_map/all_to_all | solution.py:17
  165.6 12.5 %all-gather.4 = bf16[96,2048]{1,0:T(8,128)(2,1)S(1)} all-gather(bf16[24,2048]{1,0:T(8,128)(2,1)S(1)} %get-tuple-element.9), channel_id=6, replica_groups=mesh['ep_0'=16,'ep_1'=4,'ep_2'=2,'tp'=4] {'tp'}, dimensions={0}, use_global_device_ids=true | all-gather | bytes 491520 | tf_op jit(solution)/shard_map/all_gather | solution.py:266
  178.2 2.5 %all-to-all-done.5 = bf16[16,16,512]{2,1,0:T(8,128)(2,1)S(1)} async-done(((bf16[16,16,512]{2,1,0:T(8,128)(2,1)}), bf16[16,16,512]{2,1,0:T(8,128)(2,1)S(1)}, u32[]{:S(2)}, u32[]{:S(2)}) %all-to-all-start.5) | async-done | bytes 262176 | tf_op jit(solution)/shard_map/all_to_all | solution.py:17
  181.8 3.6 %all-to-all-start.6 = ((f32[4,1,24]{2,1,0:T(1,128)}), f32[4,1,24]{2,1,0:T(1,128)S(1)}, u32[]{:S(2)}, u32[]{:S(2)}) async-start(f32[4,1,24]{2,1,0:T(1,128)} %broadcast_in_dim.80), calls=%async_computation.6 | async-start | bytes 4096 | tf_op jit(solution)/shard_map/all_to_all | solution.py:17
  185.3 5.2 %all-to-all-done.6 = f32[4,1,24]{2,1,0:T(1,128)S(1)} async-done(((f32[4,1,24]{2,1,0:T(1,128)}), f32[4,1,24]{2,1,0:T(1,128)S(1)}, u32[]{:S(2)}, u32[]{:S(2)}) %all-to-all-start.6) | async-done | bytes 416 | tf_op jit(solution)/shard_map/all_to_all | solution.py:17
  190.6 0.7 add_convert_fusion
  (75 shorter events, 5.4 us)
Async XLA Ops:
  0.6 21.6 %copy-start = (bf16[2048,128]{1,0:T(8,128)(2,1)S(1)}, bf16[2048,128]{1,0:T(8,128)(2,1)}, u32[]{:S(2)}) copy-start(bf16[2048,128]{1,0:T(8,128)(2,1)} %param.23) | copy-start | bytes 1572868
  0.6 21.6 %copy-start.14 = (f32[1,128]{1,0:T(1,128)S(1)}, f32[1,128]{1,0:T(1,128)}, u32[]{:S(2)}) copy-start(f32[1,128]{1,0:T(1,128)} %param.25) | copy-start | bytes 1540
  0.7 21.3 %copy-start.5 = (bf16[24,2048]{1,0:T(8,128)(2,1)S(1)}, bf16[24,2048]{1,0:T(8,128)(2,1)}, u32[]{:S(2)}) copy-start(bf16[24,2048]{1,0:T(8,128)(2,1)} %param.20) | copy-start | bytes 294916
  0.7 21.3 %copy-start.8 = (bf16[2048,128]{1,0:T(8,128)(2,1)S(1)}, bf16[2048,128]{1,0:T(8,128)(2,1)}, u32[]{:S(2)}) copy-start(bf16[2048,128]{1,0:T(8,128)(2,1)} %param.22) | copy-start | bytes 1572868
  0.7 21.8 %copy-start.6 = (f32[24,1,128,128]{3,2,1,0:T(8,128)S(1)}, f32[24,1,128,128]{3,2,1,0:T(8,128)}, u32[]{:S(2)}) copy-start(f32[24,1,128,128]{3,2,1,0:T(8,128)} %param.21) | copy-start | bytes 4718596
  2.3 39.3 %all-to-all-start = ((bf16[16,4,16,128]{3,2,1,0:T(8,128)(2,1)}), bf16[16,4,16,128]{3,2,1,0:T(8,128)(2,1)S(1)}, u32[]{:S(2)}, u32[]{:S(2)}) async-start(bf16[16,4,16,128]{3,2,1,0:T(8,128)(2,1)} %broadcast_in_dim.42), calls=%async_computation | async-start | bytes 524288 | tf_op jit(solution)/shard_map/all_to_all | solution.py:17
  23.6 1.1 copy-start.4
  23.6 2.7 %copy-start.9 = (s32[24,6]{0,1:T(8,128)S(1)}, s32[24,6]{0,1:T(8,128)}, u32[]{:S(2)}) copy-start(s32[24,6]{0,1:T(8,128)} %param.35) | copy-start | bytes 1732
  41.6 52.0 %copy-start.7 = (bf16[16,4,16,128]{3,2,1,0:T(8,128)(2,1)}, bf16[16,4,16,128]{3,2,1,0:T(8,128)(2,1)S(1)}, u32[]{:S(2)}) copy-start(bf16[16,4,16,128]{3,2,1,0:T(8,128)(2,1)S(1)} %all-to-all-done) | copy-start | bytes 786436
  42.6 15.2 %all-to-all-start.1 = ((bf16[32,24,128]{2,1,0:T(8,128)(2,1)}), bf16[32,24,128]{2,1,0:T(8,128)(2,1)S(1)}, u32[]{:S(2)}, u32[]{:S(2)}) async-start(bf16[32,24,128]{2,1,0:T(8,128)(2,1)} %bitcast.18), calls=%async_computation.1 | async-start | bytes 393216 | tf_op jit(solution)/shard_map/all_to_all | solution.py:17
  88.3 5.3 %copy-start.10 = (bf16[2048]{0:T(1024)(128)(2,1)S(1)}, bf16[2048]{0:T(1024)(128)(2,1)}, u32[]{:S(2)}) copy-start(bf16[2048]{0:T(1024)(128)(2,1)} %param.29) | copy-start | bytes 12292
  89.5 21.1 %copy-start.1 = (bf16[1,2048,128]{2,1,0:T(8,128)(2,1)S(1)}, bf16[1,2048,128]{2,1,0:T(8,128)(2,1)}, u32[]{:S(2)}) copy-start(bf16[1,2048,128]{2,1,0:T(8,128)(2,1)} %param.37) | copy-start | bytes 1572868
  89.5 21.1 %copy-start.2 = (bf16[1,2048,128]{2,1,0:T(8,128)(2,1)S(1)}, bf16[1,2048,128]{2,1,0:T(8,128)(2,1)}, u32[]{:S(2)}) copy-start(bf16[1,2048,128]{2,1,0:T(8,128)(2,1)} %param.38) | copy-start | bytes 1572868
  89.5 21.1 %copy-start.3 = (bf16[1,128,2048]{2,1,0:T(8,128)(2,1)S(1)}, bf16[1,128,2048]{2,1,0:T(8,128)(2,1)}, u32[]{:S(2)}) copy-start(bf16[1,128,2048]{2,1,0:T(8,128)(2,1)} %param.39) | copy-start | bytes 1572868
  89.6 21.1 %all-to-all-start.3 = ((bf16[32,32,512]{2,1,0:T(8,128)(2,1)}), bf16[32,32,512]{2,1,0:T(8,128)(2,1)S(1)}, u32[]{:S(2)}, u32[]{:S(2)}) async-start(bf16[32,32,512]{2,1,0:T(8,128)(2,1)} %bitcast.23), calls=%async_computation.3 | async-start | bytes 2097152 | tf_op jit(solution)/shard_map/all_to_all | solution.py:17
  113.5 4.1 %slice-start = ((bf16[16,4,16,128]{3,2,1,0:T(8,128)(2,1)}), bf16[16,3,16,128]{3,2,1,0:T(8,128)(2,1)S(1)}, s32[]{:S(2)}) async-start(bf16[16,4,16,128]{3,2,1,0:T(8,128)(2,1)} %copy-done.7), calls=%async_computation.7 | async-start | bytes 393216 | tf_op jit(solution)/shard_map/slice | solution.py:252
  113.6 30.9 %copy-start.11 = (bf16[2048]{0:T(1024)(128)(2,1)S(1)}, bf16[2048]{0:T(1024)(128)(2,1)}, u32[]{:S(2)}) copy-start(bf16[2048]{0:T(1024)(128)(2,1)} %param.31) | copy-start | bytes 12292
  113.6 30.9 %copy-start.12 = (f32[24,6]{0,1:T(8,128)S(1)}, f32[24,6]{0,1:T(8,128)}, u32[]{:S(2)}) copy-start(f32[24,6]{0,1:T(8,128)} %param.36) | copy-start | bytes 1732
  113.6 43.4 %all-to-all-start.4 = ((bf16[32,32,512]{2,1,0:T(8,128)(2,1)}), bf16[32,32,512]{2,1,0:T(8,128)(2,1)S(1)}, u32[]{:S(2)}, u32[]{:S(2)}) async-start(bf16[32,32,512]{2,1,0:T(8,128)(2,1)} %bitcast.28), calls=%async_computation.4 | async-start | bytes 2097152 | tf_op jit(solution)/shard_map/all_to_all | solution.py:17
  142.6 21.5 %collective-permute-start = (bf16[4,16,3,16,128]{4,3,2,1,0:T(8,128)(2,1)S(1)}, bf16[4,16,3,16,128]{4,3,2,1,0:T(8,128)(2,1)S(1)}, u32[]{:S(2)}, u32[]{:S(2)}) collective-permute-start(bf16[4,16,3,16,128]{4,3,2,1,0:T(8,128)(2,1)S(1)} %bitcast.75), channel_id=1, source_target_pairs={{0,4},{4,0},{1,5},{5,1},{2,6},{6,2},{3,7},{7,3},{8,12},{12,8},{9,1... | collective-permute-start | bytes 2359304 | tf_op jit(solution)/shard_map/ppermute | solution.py:253
  158.0 22.8 %all-to-all-start.5 = ((bf16[16,16,512]{2,1,0:T(8,128)(2,1)}), bf16[16,16,512]{2,1,0:T(8,128)(2,1)S(1)}, u32[]{:S(2)}, u32[]{:S(2)}) async-start(bf16[16,16,512]{2,1,0:T(8,128)(2,1)} %bitcast.30), calls=%async_computation.5 | async-start | bytes 524288 | tf_op jit(solution)/shard_map/all_to_all | solution.py:17
  165.0 20.3 %copy-start.13 = (bf16[512]{0:T(512)(128)(2,1)S(1)}, bf16[512]{0:T(512)(128)(2,1)}, u32[]{:S(2)}) copy-start(bf16[512]{0:T(512)(128)(2,1)} %param.30) | copy-start | bytes 3076
  181.8 8.8 %all-to-all-start.6 = ((f32[4,1,24]{2,1,0:T(1,128)}), f32[4,1,24]{2,1,0:T(1,128)S(1)}, u32[]{:S(2)}, u32[]{:S(2)}) async-start(f32[4,1,24]{2,1,0:T(1,128)} %broadcast_in_dim.80), calls=%async_computation.6 | async-start | bytes 4096 | tf_op jit(solution)/shard_map/all_to_all | solution.py:17
where the time goes:
time: 192 us; the launch traced here: 191 us
  blocking collectives  93.8 us (49%)
  starting transfers between devices  41.6 us (22%)
  waiting for transfers between devices  33.2 us (17%)
  other arithmetic  7.11 us (4%)
  Pallas kernels  6.16 us (3%)
  local copies, waits for them, and re-layouts  4.23 us (2%)
  matrix products  4.03 us (2%)
    all_to_all x6, starting transfers between devices, exchanged(): return lax.all_to_all(value, axes, 0, 0, tiled=True)  39.7 us
    all_to_all x6, waiting for transfers between devices, exchanged(): return lax.all_to_all(value, axes, 0, 0, tiled=True)  33.2 us
    all_to_all x1, blocking collectives, exchanged(): return lax.all_to_all(value, axes, 0, 0, tiled=True)  30 us
    all_gather x1, blocking collectives, shards(): shared = lax.all_gather(parts[:, 1:], 'ep_1')  24.9 us
    all_gather x1, blocking collectives, shards(): shared_terms = lax.all_gather(shared_terms, 'tp')  12.5 us
    all_gather x1, blocking collectives, shards(): heads = lax.all_gather(heads, 'ep_1').reshape(cores * seq_rows, head_dim)  12.3 us
    all_gather x1, blocking collectives, shards(): mine = lax.all_gather(resid, 'tp')  12.2 us
  transfers between devices with their start and end apart: 7, of which 4 were waited for; matrix products, arithmetic and copies ran while one was open for 5% of the time, Pallas kernels for 1%

commit v1 on v0

--- a/solution.py
+++ b/solution.py
@@ -1,3 +1,5 @@
+import functools
+
 import jax
 import jax.numpy as jnp
 from jax import lax
@@ -20,11 +22,6 @@
 def to_all(value, axes):
     devices = lax.axis_size(axes)
     return exchanged(jnp.broadcast_to(value[None], (devices, *value.shape)), axes)
-
-
-def rmsnorm(values_in, gain):
-    scale = lax.rsqrt(jnp.mean(values_in * values_in, axis=-1, keepdims=True) + epsilon)
-    return values_in * scale * gain.astype(F32)
 
 
 def from_z_order(cores, zs, inverse):
@@ -47,16 +44,92 @@
     )(*args)
 
 
-def dispatch_body(terms, places, tok, chosen, resid, send):
-    mixed = jnp.zeros(tok.shape, F32)
-    for k in range(terms.shape[0]):
+def recurrence_body(
+    tokens, gain, w_query, w_forget, w_value, floor, head_gain, state, new_hbm, out, new, read, sem
+):
+    rows = tokens.shape[0]
+    wide = tokens[...].astype(F32)
+    scale = lax.rsqrt(jnp.mean(wide * wide, axis=1, keepdims=True) + epsilon)
+    normed = (wide * scale * gain[...].astype(F32)).astype(BF)
+    query = jnp.dot(normed, w_query[...], preferred_element_type=F32)
+    query = (query * jax.nn.sigmoid(query)).T
+    pre = jnp.dot(normed, w_forget[...], preferred_element_type=F32)
+    values = jnp.dot(normed, w_value[...], preferred_element_type=F32)
+    low = floor[...]
+    forget = (low + (1.0 - low) * jax.nn.sigmoid(pre)).T
+    keys = ((1.0 - low) * jax.nn.sigmoid(-pre)).T
+    half = rows // 2
+    copies = [
+        pltpu.make_async_copy(new.at[pl.ds(k * half, half)], new_hbm.at[pl.ds(k * half, half)], sem.at[k])
+        for k in range(2)
+    ]
+    for b in range(rows):
+        fresh = forget[:, b : b + 1] * state[b] + keys[:, b : b + 1] * values[b : b + 1, :]
+        new[b] = fresh
+        read[b : b + 1, :] = jnp.sum(query[:, b : b + 1] * fresh, axis=0, keepdims=True)
+        if (b + 1) % half == 0:
+            copies[b // half].start()
+    readout = read[...]
+    scale = lax.rsqrt(jnp.mean(readout * readout, axis=1, keepdims=True) + epsilon)
+    out[...] = (readout * scale * head_gain[...].astype(F32)).astype(BF)
+    for copy in copies:
+        copy.wait()
+
+
+def recurrence_kernel(*args):
+    tokens, state = args[0], args[-1]
+    vmem = pl.BlockSpec(memory_space=pltpu.VMEM)
+    hbm = pl.BlockSpec(memory_space=pl.ANY)
+    return pl.pallas_call(
+        recurrence_body,
+        out_shape=(
+            jax.ShapeDtypeStruct(state.shape, F32),
+            jax.ShapeDtypeStruct((tokens.shape[0], state.shape[2]), BF),
+        ),
+        in_specs=[vmem] * len(args),
+        out_specs=(hbm, vmem),
+        scratch_shapes=[
+            pltpu.VMEM(state.shape, F32),
+            pltpu.VMEM((tokens.shape[0], state.shape[2]), F32),
+            pltpu.SemaphoreType.DMA((2,)),
+        ],
+        compiler_params=pltpu.CompilerParams(vmem_limit_bytes=16 * 1024 * 1024),
+        name="recurrence",
+    )(*args)
+
+
+def project_body(heads, parts, out):
+    cores, n_tp, rows, lanes = out.shape
+    n_z = parts.shape[0]
+    near = n_z // n_tp
+    acts = heads[...].reshape(cores * rows, heads.shape[2])
+    for t in range(n_tp):
+        start = t * near
+        other = (t ^ 1) * near
+        order = list(range(start, start + near)) + list(range(other, other + near))
+        columns = jnp.concatenate([parts[z, 0] for z in order], axis=0)
+        term = lax.dot_general(acts, columns, NT, preferred_element_type=F32).astype(BF)
+        out[:, t] = term.reshape(cores, rows, lanes)
+
+
+def dispatch_body(terms, tok, chosen, resid, send, *, piece):
+    cores, n_tp, rows, lanes = terms.shape
+    parts = []
+    for k in range(cores):
         part = terms[k, 0].astype(F32)
-        for t in range(1, terms.shape[1]):
+        for t in range(1, n_tp):
             part = part + terms[k, t].astype(F32)
-        mixed = mixed + jnp.dot(part.astype(BF), places[k], preferred_element_type=F32)
-    summed = (tok[...].astype(F32) + mixed).astype(BF)
-    resid[...] = summed
-    send[...] = jnp.dot(chosen[...], summed, preferred_element_type=F32).astype(BF)
+        parts.append(part.astype(BF).astype(F32))
+    owner = lax.broadcasted_iota(jnp.int32, (rows, lanes), 1) // piece
+    for z in range(tok.shape[1] // lanes):
+        mixed = jnp.zeros((rows, lanes), F32)
+        for k in range(cores):
+            turn = (k - z) * piece % lanes
+            moved = pltpu.roll(parts[k], turn, 1) if turn else parts[k]
+            mixed = jnp.where(owner == k, moved, mixed)
+        cols = pl.ds(z * lanes, lanes)
+        resid[:, cols] = (tok[:, cols].astype(F32) + mixed).astype(BF)
+    send[...] = jnp.dot(chosen[...], resid[...], preferred_element_type=F32).astype(BF)
 
 
 def spread_body(arrived, out):
@@ -190,46 +263,33 @@
     taken = (named > 0) & (rank == (column[0] % 2).astype(F32))
     chosen = jnp.where(taken, 1.0, 0.0).astype(BF).T
     combine = jnp.where(taken, jnp.sum(jnp.where(hits, route_weights[:, :, None], 0.0), axis=1), 0.0)
-    normed = rmsnorm(tokens.astype(F32), gain_mix).astype(BF)
-    queries = jax.nn.silu(jnp.dot(normed, w_query, preferred_element_type=F32))
-    forget_pre = jnp.dot(normed, w_forget, preferred_element_type=F32)
-    values_in = jnp.dot(normed, w_value, preferred_element_type=F32)
-    queries = queries.reshape(seq_rows, 1, head_dim)
-    forget_pre = forget_pre.reshape(seq_rows, 1, head_dim)
-    values_in = values_in.reshape(seq_rows, 1, head_dim)
-    forget = forget_floor + (1.0 - forget_floor) * jax.nn.sigmoid(forget_pre)
-    keys_in = (1.0 - forget_floor) * jax.nn.sigmoid(-forget_pre)
-    new_state = forget[..., None] * carried_state + keys_in[..., None] * values_in[:, :, None, :]
-    readout = jnp.einsum("bhd,bhdv->bhv", queries, new_state, precision=lax.Precision.HIGHEST)
-    head_out = rmsnorm(readout, head_gain).astype(BF).reshape(seq_rows, head_dim)
+    new_state, head_out = recurrence_kernel(
+        tokens,
+        gain_mix[None],
+        w_query,
+        w_forget,
+        w_value,
+        forget_floor,
+        head_gain,
+        carried_state.reshape(seq_rows, head_dim, head_dim),
+    )
+    new_state = new_state.reshape(carried_state.shape)
     heads = lax.all_gather(head_out, "ep_2")
-    heads = lax.all_gather(heads, "ep_1").reshape(cores * seq_rows, head_dim)
-    line_w = parts[:, 0].reshape(n_z * piece, head_dim)
-    terms = lax.dot_general(heads, line_w, NT, preferred_element_type=F32).astype(BF)
-    own = n_z * piece // n_tp
-    per = 128 // own
-    terms = terms.reshape(cores, 1, seq_rows, n_tp // per, 128)
-    terms = jnp.broadcast_to(terms, (cores, per, seq_rows, n_tp // per, 128))
-    terms = terms.transpose(0, 3, 1, 2, 4).reshape(cores * n_tp, seq_rows, 128)
-    terms = exchanged(terms, ("ep_1", "ep_2", "tp"))
-    terms = terms.reshape(cores, n_tp, seq_rows, 128)
-    core = lax.broadcasted_iota(jnp.int32, (cores, 128, slice_width), 0)
-    lane = lax.broadcasted_iota(jnp.int32, (cores, 128, slice_width), 1) - own * (here % per)
-    target = lax.broadcasted_iota(jnp.int32, (cores, 128, slice_width), 2)
-    places = (
-        (lane >= 0)
-        & (lane < own)
-        & (target == (lane // piece * cores + core) * piece + lane % piece)
-    )
-    places = jnp.where(places, 1.0, 0.0).astype(BF)
+    heads = lax.all_gather(heads, "ep_1").reshape(cores, seq_rows, head_dim)
+    terms = vmem_call(
+        project_body, jax.ShapeDtypeStruct((cores, n_tp, seq_rows, 128), BF), (heads, parts)
+    )
+    terms = exchanged(
+        terms.reshape(cores * n_tp, seq_rows, 128), ("ep_1", "ep_2", "tp")
+    ).reshape(terms.shape)
     token_slice = lax.dynamic_slice_in_dim(tokens, here * slice_width, slice_width, 1)
     resid, send = vmem_call(
-        dispatch_body,
+        functools.partial(dispatch_body, piece=piece),
         (
             jax.ShapeDtypeStruct((seq_rows, slice_width), BF),
             jax.ShapeDtypeStruct((slots_all, slice_width), BF),
         ),
-        (terms, places, token_slice, chosen),
+        (terms, token_slice, chosen),
     )
     arrived = exchanged(send.reshape(n_z, 2 * cores, slice_width), "ep_0")
     mine = lax.all_gather(resid, "tp")

time: 192 us -> 194 us (1.010)
  local copies, waits for them, and re-layouts: 4.23 us -> 10.4 us
  Pallas kernels: 6.16 us -> 9.72 us
  matrix products: 4.03 us -> 0.59 us
  other arithmetic: 7.11 us -> 3.77 us
    unnamed x30 -> x32, local copies, waits for them, and re-layouts: 1.2 us -> 6.77 us
    dot_general x5 -> x0, matrix products: 3.43 us -> none  [the longest x1 1.41 us: shards(): jnp.einsum('bhd,bhdv->bhv', queries, new_state, precision=lax.Precision.H...]
    pallas_call x0 -> x1, Pallas kernels: none -> 2.81 us  [recurrence_kernel(): pl.pallas_call(recurrence_body, out_shape=(jax.ShapeDtypeStruct(state.sha...]
    pallas_call x4 -> x5, Pallas kernels: 3.31 us -> 4.06 us  [vmem_call(): pl.pallas_call(body, out_shape=out_shape, in_specs=[vmem] * len(args), ou...]
  transfers between devices with their start and end apart: 7 -> 7, of which waited for: 4 -> 4; matrix products, arithmetic and copies ran while one was open for 5% -> 3% of each run, Pallas kernels for 1% -> 2%
where the time goes in v1:
time: 194 us; the launch traced here: 192 us
  blocking collectives  93.8 us (48%)
  starting transfers between devices  41.6 us (21%)
  waiting for transfers between devices  31.6 us (16%)
  local copies, waits for them, and re-layouts  10.4 us (5%)
  Pallas kernels  9.72 us (5%)
  other arithmetic  3.77 us (2%)
    all_to_all x6, starting transfers between devices, exchanged(): return lax.all_to_all(value, axes, 0, 0, tiled=True)  39.7 us
    all_to_all x6, waiting for transfers between devices, exchanged(): return lax.all_to_all(value, axes, 0, 0, tiled=True)  31.6 us
    all_to_all x1, blocking collectives, exchanged(): return lax.all_to_all(value, axes, 0, 0, tiled=True)  30 us
    all_gather x1, blocking collectives, shards(): shared = lax.all_gather(parts[:, 1:], 'ep_1')  24.8 us
    all_gather x1, blocking collectives, shards(): shared_terms = lax.all_gather(shared_terms, 'tp')  12.5 us
    all_gather x1, blocking collectives, shards(): heads = lax.all_gather(heads, 'ep_1').reshape(cores, seq_rows, head_dim)  12.3 us
    all_gather x1, blocking collectives, shards(): mine = lax.all_gather(resid, 'tp')  12.2 us
    unnamed x32, local copies, waits for them, and re-layouts  6.77 us
  transfers between devices with their start and end apart: 7, of which 4 were waited for; matrix products, arithmetic and copies ran while one was open for 3% of the time, Pallas kernels for 2%

profile of v1, /device:TPU:32, one launch (start us, length us, event | category | flops | bytes accessed | tf_op | source)
XLA Modules:
  0.0 192.4 jit_solution(17766050581339518232)
XLA Ops:
  0.6 0.7 pad_maximum_fusion
  1.4 0.7 broadcast_in_dim.49
  2.1 15.2 %all-to-all-start = ((bf16[16,4,16,128]{3,2,1,0:T(8,128)(2,1)}), bf16[16,4,16,128]{3,2,1,0:T(8,128)(2,1)S(1)}, u32[]{:S(2)}, u32[]{:S(2)}) async-start(bf16[16,4,16,128]{3,2,1,0:T(8,128)(2,1)} %broadcast_in_dim.49), calls=%async_computation | async-start | bytes 524288 | tf_op jit(solution)/shard_map/all_to_all | solution.py:19
  18.0 0.8 compare_reduce_fusion
  18.9 1.4 copy-done.1
  20.3 1.0 copy-done.5
  21.4 1.0 copy-done.6
  22.4 1.0 copy-done.7
  23.5 0.9 copy-done.8
  25.7 2.8 %recurrence.1 = (f32[24,128,128]{2,1,0:T(8,128)}, bf16[24,128]{1,0:T(8,128)(2,1)S(1)}) custom-call(bf16[24,2048]{1,0:T(8,128)(2,1)S(1)} %copy-done.8, bf16[1,2048]{1,0:T(2,128)(2,1)S(1)} %broadcast_in_dim.48.gain, bf16[2048,128]{1,0:T(8,128)(2,1)S(1)} %copy-done.5, bf16[2048,128]{1,0:T(8,128)(2,1)S(1)} %copy-done.6, bf16[2048,128]{1,0:T(8,128)(2,1)S(1)} %copy-done.7, ...), custom_call_target="tpu_custom_call" | custom-call | tf_op jit(solution)/shard_map/recurrence/pallas_call | solution.py:83
  28.5 1.8 all-gather
  30.3 12.3 %all-gather.1.heads = bf16[8,24,128]{2,1,0:T(8,128)(2,1)S(1)} all-gather(bf16[2,24,128]{2,1,0:T(8,128)(2,1)S(1)} %bitcast.62), channel_id=3, replica_groups=mesh['ep_0'=16,'ep_1'=4,'ep_2'=2,'tp'=4] {'ep_1'}, dimensions={0}, use_global_device_ids=true | all-gather | bytes 61440 | tf_op jit(solution)/shard_map/all_gather | solution.py:278
  42.8 0.9 shard_map.203
  43.7 6.7 %all-to-all-start.1 = ((bf16[32,24,128]{2,1,0:T(8,128)(2,1)}), bf16[32,24,128]{2,1,0:T(8,128)(2,1)S(1)}, u32[]{:S(2)}, u32[]{:S(2)}) async-start(bf16[32,24,128]{2,1,0:T(8,128)(2,1)} %bitcast.8), calls=%async_computation.1 | async-start | bytes 393216 | tf_op jit(solution)/shard_map/all_to_all | solution.py:19
  50.4 0.7 constant_dynamic-slice_fusion.tok
  51.2 7.7 %all-to-all-done.1 = bf16[32,24,128]{2,1,0:T(8,128)(2,1)S(1)} async-done(((bf16[32,24,128]{2,1,0:T(8,128)(2,1)}), bf16[32,24,128]{2,1,0:T(8,128)(2,1)S(1)}, u32[]{:S(2)}, u32[]{:S(2)}) %all-to-all-start.1) | async-done | bytes 196640 | tf_op jit(solution)/shard_map/all_to_all | solution.py:19
  59.2 30.0 %all_to_all.36 = bf16[16,16,512]{2,1,0:T(8,128)(2,1)S(1)} all-to-all(bf16[16,16,512]{2,1,0:T(8,128)(2,1)S(1)} %bitcast.57), channel_id=1, replica_groups=mesh['ep_0'=16,'ep_1'=4,'ep_2'=2,'tp'=4] {'ep_0'}, dimensions={0} | all-to-all | bytes 524288 | tf_op jit(solution)/shard_map/all_to_all | solution.py:19
  89.3 1.2 shard_map.205
  90.5 4.1 %all-to-all-start.3 = ((bf16[32,32,512]{2,1,0:T(8,128)(2,1)}), bf16[32,32,512]{2,1,0:T(8,128)(2,1)S(1)}, u32[]{:S(2)}, u32[]{:S(2)}) async-start(bf16[32,32,512]{2,1,0:T(8,128)(2,1)} %bitcast.13), calls=%async_computation.3 | async-start | bytes 2097152 | tf_op jit(solution)/shard_map/all_to_all | solution.py:19
  94.6 17.0 %all-to-all-done.3 = bf16[32,32,512]{2,1,0:T(8,128)(2,1)S(1)} async-done(((bf16[32,32,512]{2,1,0:T(8,128)(2,1)}), bf16[32,32,512]{2,1,0:T(8,128)(2,1)S(1)}, u32[]{:S(2)}, u32[]{:S(2)}) %all-to-all-start.3) | async-done | bytes 1048608 | tf_op jit(solution)/shard_map/all_to_all | solution.py:19
  111.6 2.9 %expert.1 = bf16[8,4,32,512]{3,2,1,0:T(8,128)(2,1)} custom-call(bf16[8,4,32,512]{3,2,1,0:T(8,128)(2,1)S(1)} %bitcast.45, bf16[1,2048]{1,0:T(2,128)(2,1)S(1)} %broadcast_in_dim.54.gain, bf16[2048,128]{1,0:T(8,128)(2,1)S(1)} %bitcast.53, bf16[2048,128]{1,0:T(8,128)(2,1)S(1)} %bitcast.54, bf16[128,2048]{1,0:T(8,128)(2,1)S(1)} %bitcast.55), custom_call_target="tpu_custom_call" | custom-call | tf_op jit(solution)/shard_map/expert/pallas_call | solution.py:194
  114.5 4.1 %all-to-all-start.4 = ((bf16[32,32,512]{2,1,0:T(8,128)(2,1)}), bf16[32,32,512]{2,1,0:T(8,128)(2,1)S(1)}, u32[]{:S(2)}, u32[]{:S(2)}) async-start(bf16[32,32,512]{2,1,0:T(8,128)(2,1)} %bitcast.18), calls=%async_computation.4 | async-start | bytes 2097152 | tf_op jit(solution)/shard_map/all_to_all | solution.py:19
  118.6 24.8 %all-gather.3 = bf16[64,3,16,128]{3,2,1,0:T(8,128)(2,1)S(1)} all-gather(bf16[16,3,16,128]{3,2,1,0:T(8,128)(2,1)S(1)} %slice-done), channel_id=5, replica_groups=mesh['ep_0'=16,'ep_1'=4,'ep_2'=2,'tp'=4] {'ep_1'}, dimensions={0}, use_global_device_ids=true | all-gather | bytes 983040 | tf_op jit(solution)/shard_map/all_gather | solution.py:312
  143.7 1.9 collective-permute-start
  145.9 12.2 %all-gather.2 = bf16[96,512]{1,0:T(8,128)(2,1)S(1)} all-gather(bf16[24,512]{1,0:T(8,128)(2,1)S(1)} %get-tuple-element.9), channel_id=4, replica_groups=mesh['ep_0'=16,'ep_1'=4,'ep_2'=2,'tp'=4] {'tp'}, dimensions={0}, use_global_device_ids=true | all-gather | bytes 122880 | tf_op jit(solution)/shard_map/all_gather | solution.py:295
  158.2 1.0 shard_map.206
  159.2 6.1 %all-to-all-start.5 = ((bf16[16,16,512]{2,1,0:T(8,128)(2,1)}), bf16[16,16,512]{2,1,0:T(8,128)(2,1)S(1)}, u32[]{:S(2)}, u32[]{:S(2)}) async-start(bf16[16,16,512]{2,1,0:T(8,128)(2,1)} %bitcast.20), calls=%async_computation.5 | async-start | bytes 524288 | tf_op jit(solution)/shard_map/all_to_all | solution.py:19
  165.3 1.2 select_bitcast_fusion.1
  167.6 12.5 %all-gather.4 = bf16[96,2048]{1,0:T(8,128)(2,1)S(1)} all-gather(bf16[24,2048]{1,0:T(8,128)(2,1)S(1)} %get-tuple-element.12), channel_id=6, replica_groups=mesh['ep_0'=16,'ep_1'=4,'ep_2'=2,'tp'=4] {'tp'}, dimensions={0}, use_global_device_ids=true | all-gather | bytes 491520 | tf_op jit(solution)/shard_map/all_gather | solution.py:326
  180.3 1.7 all-to-all-done.5
  182.9 3.6 %all-to-all-start.6 = ((f32[4,1,24]{2,1,0:T(1,128)}), f32[4,1,24]{2,1,0:T(1,128)S(1)}, u32[]{:S(2)}, u32[]{:S(2)}) async-start(f32[4,1,24]{2,1,0:T(1,128)} %broadcast_in_dim.56), calls=%async_computation.6 | async-start | bytes 4096 | tf_op jit(solution)/shard_map/all_to_all | solution.py:19
  186.5 5.2 %all-to-all-done.6 = f32[4,1,24]{2,1,0:T(1,128)S(1)} async-done(((f32[4,1,24]{2,1,0:T(1,128)}), f32[4,1,24]{2,1,0:T(1,128)S(1)}, u32[]{:S(2)}, u32[]{:S(2)}) %all-to-all-start.6) | async-done | bytes 416 | tf_op jit(solution)/shard_map/all_to_all | solution.py:19
  (55 shorter events, 6.0 us)
Async XLA Ops:
  2.1 40.7 %all-to-all-start = ((bf16[16,4,16,128]{3,2,1,0:T(8,128)(2,1)}), bf16[16,4,16,128]{3,2,1,0:T(8,128)(2,1)S(1)}, u32[]{:S(2)}, u32[]{:S(2)}) async-start(bf16[16,4,16,128]{3,2,1,0:T(8,128)(2,1)} %broadcast_in_dim.49), calls=%async_computation | async-start | bytes 524288 | tf_op jit(solution)/shard_map/all_to_all | solution.py:19
  18.9 1.4 copy-start.1
  20.3 1.0 copy-start.5
  21.4 1.0 copy-start.6
  22.4 1.0 copy-start.7
  23.5 0.9 copy-start.8
  24.4 0.7 copy-start.9
  25.0 0.7 copy-start.10
  42.8 51.8 %copy-start = (bf16[16,4,16,128]{3,2,1,0:T(8,128)(2,1)}, bf16[16,4,16,128]{3,2,1,0:T(8,128)(2,1)S(1)}, u32[]{:S(2)}) copy-start(bf16[16,4,16,128]{3,2,1,0:T(8,128)(2,1)S(1)} %all-to-all-done.parts) | copy-start | bytes 786436
  43.7 15.2 %all-to-all-start.1 = ((bf16[32,24,128]{2,1,0:T(8,128)(2,1)}), bf16[32,24,128]{2,1,0:T(8,128)(2,1)S(1)}, u32[]{:S(2)}, u32[]{:S(2)}) async-start(bf16[32,24,128]{2,1,0:T(8,128)(2,1)} %bitcast.8), calls=%async_computation.1 | async-start | bytes 393216 | tf_op jit(solution)/shard_map/all_to_all | solution.py:19
  89.3 5.3 %copy-start.12 = (bf16[2048]{0:T(1024)(128)(2,1)S(1)}, bf16[2048]{0:T(1024)(128)(2,1)}, u32[]{:S(2)}) copy-start(bf16[2048]{0:T(1024)(128)(2,1)} %param.29) | copy-start | bytes 12292
  90.5 21.1 %copy-start.2 = (bf16[1,2048,128]{2,1,0:T(8,128)(2,1)S(1)}, bf16[1,2048,128]{2,1,0:T(8,128)(2,1)}, u32[]{:S(2)}) copy-start(bf16[1,2048,128]{2,1,0:T(8,128)(2,1)} %param.37) | copy-start | bytes 1572868
  90.5 21.1 %copy-start.3 = (bf16[1,2048,128]{2,1,0:T(8,128)(2,1)S(1)}, bf16[1,2048,128]{2,1,0:T(8,128)(2,1)}, u32[]{:S(2)}) copy-start(bf16[1,2048,128]{2,1,0:T(8,128)(2,1)} %param.38) | copy-start | bytes 1572868
  90.5 21.1 %copy-start.4 = (bf16[1,128,2048]{2,1,0:T(8,128)(2,1)S(1)}, bf16[1,128,2048]{2,1,0:T(8,128)(2,1)}, u32[]{:S(2)}) copy-start(bf16[1,128,2048]{2,1,0:T(8,128)(2,1)} %param.39) | copy-start | bytes 1572868
  90.5 21.1 %all-to-all-start.3 = ((bf16[32,32,512]{2,1,0:T(8,128)(2,1)}), bf16[32,32,512]{2,1,0:T(8,128)(2,1)S(1)}, u32[]{:S(2)}, u32[]{:S(2)}) async-start(bf16[32,32,512]{2,1,0:T(8,128)(2,1)} %bitcast.13), calls=%async_computation.3 | async-start | bytes 2097152 | tf_op jit(solution)/shard_map/all_to_all | solution.py:19
  114.5 4.1 %slice-start = ((bf16[16,4,16,128]{3,2,1,0:T(8,128)(2,1)}), bf16[16,3,16,128]{3,2,1,0:T(8,128)(2,1)S(1)}, s32[]{:S(2)}) async-start(bf16[16,4,16,128]{3,2,1,0:T(8,128)(2,1)} %copy-done), calls=%async_computation.7 | async-start | bytes 393216 | tf_op jit(solution)/shard_map/slice | solution.py:312
  114.5 43.6 %all-to-all-start.4 = ((bf16[32,32,512]{2,1,0:T(8,128)(2,1)}), bf16[32,32,512]{2,1,0:T(8,128)(2,1)S(1)}, u32[]{:S(2)}, u32[]{:S(2)}) async-start(bf16[32,32,512]{2,1,0:T(8,128)(2,1)} %bitcast.18), calls=%async_computation.4 | async-start | bytes 2097152 | tf_op jit(solution)/shard_map/all_to_all | solution.py:19
  118.6 27.1 %copy-start.13 = (bf16[2048]{0:T(1024)(128)(2,1)S(1)}, bf16[2048]{0:T(1024)(128)(2,1)}, u32[]{:S(2)}) copy-start(bf16[2048]{0:T(1024)(128)(2,1)} %param.31) | copy-start | bytes 12292
  118.6 27.1 %copy-start.11 = (s32[24,6]{0,1:T(8,128)S(1)}, s32[24,6]{0,1:T(8,128)}, u32[]{:S(2)}) copy-start(s32[24,6]{0,1:T(8,128)} %param.35) | copy-start | bytes 1732
  118.6 27.1 %copy-start.14 = (f32[24,6]{0,1:T(8,128)S(1)}, f32[24,6]{0,1:T(8,128)}, u32[]{:S(2)}) copy-start(f32[24,6]{0,1:T(8,128)} %param.36) | copy-start | bytes 1732
  143.7 21.6 %collective-permute-start = (bf16[4,16,3,16,128]{4,3,0,1,2:T(8,128)(2,1)S(1)}, bf16[4,16,3,16,128]{4,3,0,1,2:T(8,128)(2,1)}, u32[]{:S(2)}, u32[]{:S(2)}) collective-permute-start(bf16[4,16,3,16,128]{4,3,0,1,2:T(8,128)(2,1)S(1)} %copy.58), channel_id=1, source_target_pairs={{0,4},{4,0},{1,5},{5,1},{2,6},{6,2},{3,7},{7,3},{8,12},{12,8},{9,1... | collective-permute-start | bytes 2359304 | tf_op jit(solution)/shard_map/ppermute | solution.py:313
  159.2 22.8 %all-to-all-start.5 = ((bf16[16,16,512]{2,1,0:T(8,128)(2,1)}), bf16[16,16,512]{2,1,0:T(8,128)(2,1)S(1)}, u32[]{:S(2)}, u32[]{:S(2)}) async-start(bf16[16,16,512]{2,1,0:T(8,128)(2,1)} %bitcast.20), calls=%async_computation.5 | async-start | bytes 524288 | tf_op jit(solution)/shard_map/all_to_all | solution.py:19
  167.0 19.5 %copy-start.15 = (bf16[512]{0:T(512)(128)(2,1)S(1)}, bf16[512]{0:T(512)(128)(2,1)}, u32[]{:S(2)}) copy-start(bf16[512]{0:T(512)(128)(2,1)} %param.30) | copy-start | bytes 3076
  182.9 8.8 %all-to-all-start.6 = ((f32[4,1,24]{2,1,0:T(1,128)}), f32[4,1,24]{2,1,0:T(1,128)S(1)}, u32[]{:S(2)}, u32[]{:S(2)}) async-start(f32[4,1,24]{2,1,0:T(1,128)} %broadcast_in_dim.56), calls=%async_computation.6 | async-start | bytes 4096 | tf_op jit(solution)/shard_map/all_to_all | solution.py:19

commit v2 on v0

--- a/solution.py
+++ b/solution.py
@@ -1,3 +1,5 @@
+import functools
+
 import jax
 import jax.numpy as jnp
 from jax import lax
@@ -20,6 +22,12 @@
 def to_all(value, axes):
     devices = lax.axis_size(axes)
     return exchanged(jnp.broadcast_to(value[None], (devices, *value.shape)), axes)
+
+
+def turned(value, step, devices):
+    if step == 0:
+        return value
+    return lax.ppermute(value, "tp", [(k, (k + step) % devices) for k in range(devices)])
 
 
 def rmsnorm(values_in, gain):
@@ -47,16 +55,38 @@
     )(*args)
 
 
-def dispatch_body(terms, places, tok, chosen, resid, send):
-    mixed = jnp.zeros(tok.shape, F32)
-    for k in range(terms.shape[0]):
+def project_body(heads, parts, out):
+    cores, n_tp, rows, lanes = out.shape
+    n_z = parts.shape[0]
+    near = n_z // n_tp
+    acts = heads[...].reshape(cores * rows, heads.shape[2])
+    for t in range(n_tp):
+        start = t * near
+        other = (t ^ 1) * near
+        order = list(range(start, start + near)) + list(range(other, other + near))
+        columns = jnp.concatenate([parts[z, 0] for z in order], axis=0)
+        term = lax.dot_general(acts, columns, NT, preferred_element_type=F32).astype(BF)
+        out[:, t] = term.reshape(cores, rows, lanes)
+
+
+def dispatch_body(terms, tok, chosen, resid, send, *, piece):
+    cores, n_tp, rows, lanes = terms.shape
+    parts = []
+    for k in range(cores):
         part = terms[k, 0].astype(F32)
-        for t in range(1, terms.shape[1]):
+        for t in range(1, n_tp):
             part = part + terms[k, t].astype(F32)
-        mixed = mixed + jnp.dot(part.astype(BF), places[k], preferred_element_type=F32)
-    summed = (tok[...].astype(F32) + mixed).astype(BF)
-    resid[...] = summed
-    send[...] = jnp.dot(chosen[...], summed, preferred_element_type=F32).astype(BF)
+        parts.append(part.astype(BF).astype(F32))
+    owner = lax.broadcasted_iota(jnp.int32, (rows, lanes), 1) // piece
+    for z in range(tok.shape[1] // lanes):
+        mixed = jnp.zeros((rows, lanes), F32)
+        for k in range(cores):
+            turn = (k - z) * piece % lanes
+            moved = pltpu.roll(parts[k], turn, 1) if turn else parts[k]
+            mixed = jnp.where(owner == k, moved, mixed)
+        cols = pl.ds(z * lanes, lanes)
+        resid[:, cols] = (tok[:, cols].astype(F32) + mixed).astype(BF)
+    send[...] = jnp.dot(chosen[...], resid[...], preferred_element_type=F32).astype(BF)
 
 
 def spread_body(arrived, out):
@@ -135,15 +165,49 @@
     )(x, gain, gate_w, up_w, down_w)
 
 
-def shared_body(x, gain, mix_w, gate_w, up_w, down_w, out, mix, hn):
-    n_tp = x.shape[0]
-    normed_columns((n_tp, lambda j: x[j]), gain, hn)
-    logits = jnp.sum(hn[...].astype(F32) * mix_w[...].astype(F32), axis=1, keepdims=True)
+def shared_body(place, x, gain, mix_w, gate_w, up_w, down_w, out, mix):
+    n_tp, rows, slice_width = x.shape
+    here = place[0]
+    squares = jnp.zeros((rows, 1), F32)
+    for k in range(n_tp):
+        wide = x[k].astype(F32)
+        squares = squares + jnp.sum(wide * wide, axis=1, keepdims=True)
+    scale = lax.rsqrt(squares / (n_tp * slice_width) + epsilon)
+    logits = jnp.zeros((rows, 1), F32)
+    gate_pre = jnp.zeros((rows, gate_w.shape[1]), F32)
+    up_pre = jnp.zeros((rows, up_w.shape[1]), F32)
+    for k in range(n_tp):
+        j = lax.rem(here + (n_tp - k), n_tp)
+        cols = pl.ds(pl.multiple_of(j * slice_width, slice_width), slice_width)
+        part = (x[k].astype(F32) * scale * gain[pl.ds(j, 1), :].astype(F32)).astype(BF)
+        logits = logits + jnp.sum(
+            part.astype(F32) * mix_w[pl.ds(j, 1), :].astype(F32), axis=1, keepdims=True
+        )
+        gate_pre = gate_pre + jnp.dot(part, gate_w[cols, :], preferred_element_type=F32)
+        up_pre = up_pre + jnp.dot(part, up_w[cols, :], preferred_element_type=F32)
     mix[...] = jnp.broadcast_to(jax.nn.sigmoid(logits), mix.shape)
-    gate_pre = jnp.dot(hn[...], gate_w[...], preferred_element_type=F32)
-    up_pre = jnp.dot(hn[...], up_w[...], preferred_element_type=F32)
     hidden = (gate_pre * jax.nn.sigmoid(gate_pre) * up_pre).astype(BF)
-    out[...] = lax.dot_general(hidden, down_w[...], NT, preferred_element_type=F32).astype(BF)
+    for k in range(n_tp):
+        j = lax.rem(here + k, n_tp)
+        cols = pl.ds(pl.multiple_of(j * slice_width, slice_width), slice_width)
+        out[k] = lax.dot_general(hidden, down_w[cols, :], NT, preferred_element_type=F32).astype(BF)
+
+
+def shared_kernel(place, *args):
+    n_tp, rows, slice_width = args[0].shape
+    vmem = pl.BlockSpec(memory_space=pltpu.VMEM)
+    smem = pl.BlockSpec(memory_space=pltpu.SMEM)
+    return pl.pallas_call(
+        shared_body,
+        out_shape=(
+            jax.ShapeDtypeStruct((n_tp, rows, slice_width), BF),
+            jax.ShapeDtypeStruct((rows, 128), F32),
+        ),
+        in_specs=[smem] + [vmem] * len(args),
+        out_specs=(vmem, vmem),
+        compiler_params=pltpu.CompilerParams(vmem_limit_bytes=16 * 1024 * 1024),
+        name="shared",
+    )(place, *args)
 
 
 def shards(
@@ -202,37 +266,25 @@
     new_state = forget[..., None] * carried_state + keys_in[..., None] * values_in[:, :, None, :]
     readout = jnp.einsum("bhd,bhdv->bhv", queries, new_state, precision=lax.Precision.HIGHEST)
     head_out = rmsnorm(readout, head_gain).astype(BF).reshape(seq_rows, head_dim)
-    heads = lax.all_gather(head_out, "ep_2")
-    heads = lax.all_gather(heads, "ep_1").reshape(cores * seq_rows, head_dim)
-    line_w = parts[:, 0].reshape(n_z * piece, head_dim)
-    terms = lax.dot_general(heads, line_w, NT, preferred_element_type=F32).astype(BF)
-    own = n_z * piece // n_tp
-    per = 128 // own
-    terms = terms.reshape(cores, 1, seq_rows, n_tp // per, 128)
-    terms = jnp.broadcast_to(terms, (cores, per, seq_rows, n_tp // per, 128))
-    terms = terms.transpose(0, 3, 1, 2, 4).reshape(cores * n_tp, seq_rows, 128)
-    terms = exchanged(terms, ("ep_1", "ep_2", "tp"))
-    terms = terms.reshape(cores, n_tp, seq_rows, 128)
-    core = lax.broadcasted_iota(jnp.int32, (cores, 128, slice_width), 0)
-    lane = lax.broadcasted_iota(jnp.int32, (cores, 128, slice_width), 1) - own * (here % per)
-    target = lax.broadcasted_iota(jnp.int32, (cores, 128, slice_width), 2)
-    places = (
-        (lane >= 0)
-        & (lane < own)
-        & (target == (lane // piece * cores + core) * piece + lane % piece)
-    )
-    places = jnp.where(places, 1.0, 0.0).astype(BF)
+    head_out, parts = lax.optimization_barrier((head_out, parts))
+    heads = to_all(head_out, ("ep_1", "ep_2"))
+    terms = vmem_call(
+        project_body, jax.ShapeDtypeStruct((cores, n_tp, seq_rows, 128), BF), (heads, parts)
+    )
+    terms = exchanged(
+        terms.reshape(cores * n_tp, seq_rows, 128), ("ep_1", "ep_2", "tp")
+    ).reshape(terms.shape)
     token_slice = lax.dynamic_slice_in_dim(tokens, here * slice_width, slice_width, 1)
     resid, send = vmem_call(
-        dispatch_body,
+        functools.partial(dispatch_body, piece=piece),
         (
             jax.ShapeDtypeStruct((seq_rows, slice_width), BF),
             jax.ShapeDtypeStruct((slots_all, slice_width), BF),
         ),
-        (terms, places, token_slice, chosen),
+        (terms, token_slice, chosen),
     )
     arrived = exchanged(send.reshape(n_z, 2 * cores, slice_width), "ep_0")
-    mine = lax.all_gather(resid, "tp")
+    mine = jnp.stack([turned(resid, k, n_tp) for k in range(n_tp)])
     spread = vmem_call(
         spread_body,
         jax.ShapeDtypeStruct((cores, n_tp, 2 * n_z, slice_width), BF),
@@ -254,18 +306,17 @@
     first = lax.axis_index("ep_2") == 0
     shared = jnp.stack([jnp.where(first, shared, other), jnp.where(first, other, shared)])
     shared = shared.transpose(3, 2, 1, 0, 4, 5).reshape(3, model_width, head_dim)
-    shared_terms, mix = vmem_call(
-        shared_body,
-        (
-            jax.ShapeDtypeStruct((seq_rows, model_width), BF),
-            jax.ShapeDtypeStruct((seq_rows, 128), F32),
-        ),
-        (mine, gain_ffn[None], w_branch_gate[None], shared[0], shared[1], shared[2]),
-        (pltpu.VMEM((seq_rows, model_width), BF),),
-    )
-    shared_terms = lax.all_gather(shared_terms, "tp")
-    shared_terms = lax.dynamic_slice_in_dim(shared_terms, here * slice_width, slice_width, 2)
-    shared_out = jnp.sum(shared_terms.astype(F32), axis=0).astype(BF)
+    shared_terms, mix = shared_kernel(
+        here.astype(jnp.int32)[None],
+        mine,
+        gain_ffn.reshape(n_tp, slice_width).astype(F32),
+        w_branch_gate.reshape(n_tp, slice_width).astype(F32),
+        shared[0],
+        shared[1],
+        shared[2],
+    )
+    shared_parts = [turned(shared_terms[k], k, n_tp) for k in range(n_tp)]
+    shared_out = sum(p.astype(F32) for p in shared_parts).astype(BF)
     routed = jnp.dot(combine, returned.astype(F32), precision=lax.Precision.HIGHEST)
     branch_sum = routed + mix[:, :1] * shared_out.astype(F32)
     square_part = jnp.sum(branch_sum * branch_sum, axis=1)

time: 192 us -> 192 us (level)
  blocking collectives: 93.8 us -> 49.1 us
  starting transfers between devices: 41.6 us -> 66.3 us
  waiting for transfers between devices: 33.2 us -> 53.4 us
    all_gather x4 -> x0, blocking collectives: 38.9 us -> none  [the longest x1 12.5 us: shards(): shared_terms = lax.all_gather(shared_terms, 'tp')]
    ppermute x0 -> x6, starting transfers between devices: none -> 21.2 us  [turned(): lax.ppermute(value, 'tp', [(k, (k + step) % devices) for k in range(devic...]
    all_to_all x6 -> x7, waiting for transfers between devices: 33.2 us -> 48.3 us  [exchanged(): return lax.all_to_all(value, axes, 0, 0, tiled=True)]
    all_to_all x1, blocking collectives: 30 us -> 24.3 us  [exchanged(): return lax.all_to_all(value, axes, 0, 0, tiled=True)]
    ppermute x0 -> x6, waiting for transfers between devices: none -> 5.08 us  [turned(): lax.ppermute(value, 'tp', [(k, (k + step) % devices) for k in range(devic...]
    all_to_all x6 -> x7, starting transfers between devices: 39.7 us -> 43.1 us  [exchanged(): return lax.all_to_all(value, axes, 0, 0, tiled=True)]
  transfers between devices with their start and end apart: 7 -> 14, of which waited for: 4 -> 8; matrix products, arithmetic and copies ran while one was open for 5% -> 5% of each run, Pallas kernels for 1% -> 1%
where the time goes in v2:
time: 192 us; the launch traced here: 191 us
  starting transfers between devices  66.3 us (35%)
  waiting for transfers between devices  53.4 us (28%)
  blocking collectives  49.1 us (26%)
  Pallas kernels  7 us (4%)
  other arithmetic  6.83 us (4%)
  matrix products  3.86 us (2%)
  local copies, waits for them, and re-layouts  3.74 us (2%)
    all_to_all x7, waiting for transfers between devices, exchanged(): return lax.all_to_all(value, axes, 0, 0, tiled=True)  48.3 us
    all_to_all x7, starting transfers between devices, exchanged(): return lax.all_to_all(value, axes, 0, 0, tiled=True)  43.1 us
    all_gather x1, blocking collectives, shards(): shared = lax.all_gather(parts[:, 1:], 'ep_1')  24.9 us
    all_to_all x1, blocking collectives, exchanged(): return lax.all_to_all(value, axes, 0, 0, tiled=True)  24.3 us
    ppermute x6, starting transfers between devices, turned(): lax.ppermute(value, 'tp', [(k, (k + step) % devices) for k in range(devic...  21.2 us
    ppermute x6, waiting for transfers between devices, turned(): lax.ppermute(value, 'tp', [(k, (k + step) % devices) for k in range(devic...  5.08 us
  transfers between devices with their start and end apart: 14, of which 8 were waited for; matrix products, arithmetic and copies ran while one was open for 5% of the time, Pallas kernels for 1%

profile of v2, /device:TPU:32, one launch (start us, length us, event | category | flops | bytes accessed | tf_op | source)
XLA Modules:
  0.0 191.4 jit_solution(5376873651583642755)
XLA Ops:
  2.3 15.2 %all-to-all-start = ((bf16[16,4,16,128]{3,2,1,0:T(8,128)(2,1)}), bf16[16,4,16,128]{3,2,1,0:T(8,128)(2,1)S(1)}, u32[]{:S(2)}, u32[]{:S(2)}) async-start(bf16[16,4,16,128]{3,2,1,0:T(8,128)(2,1)} %broadcast_in_dim.32), calls=%async_computation | async-start | bytes 524288 | tf_op jit(solution)/shard_map/all_to_all | solution.py:19
  18.3 1.0 fusion.3
  20.0 1.3 fusion.18
  22.1 1.0 multiply_add_fusion
  23.2 1.4 fusion
  24.8 10.6 %all-to-all-done.parts = bf16[16,4,16,128]{3,2,1,0:T(8,128)(2,1)S(1)} async-done(((bf16[16,4,16,128]{3,2,1,0:T(8,128)(2,1)}), bf16[16,4,16,128]{3,2,1,0:T(8,128)(2,1)S(1)}, u32[]{:S(2)}, u32[]{:S(2)}) %all-to-all-start) | async-done | bytes 262176 | tf_op jit(solution)/shard_map/all_to_all | solution.py:19
  36.1 4.3 %all-to-all-start.1 = ((bf16[8,24,128]{2,1,0:T(8,128)(2,1)}), bf16[8,24,128]{2,1,0:T(8,128)(2,1)S(1)}, u32[]{:S(2)}, u32[]{:S(2)}) async-start(bf16[8,24,128]{2,1,0:T(8,128)(2,1)} %broadcast_in_dim.33), calls=%async_computation.1 | async-start | bytes 98304 | tf_op jit(solution)/shard_map/all_to_all | solution.py:19
  40.7 5.3 %all-to-all-done.1.heads = bf16[8,24,128]{2,1,0:T(8,128)(2,1)S(1)} async-done(((bf16[8,24,128]{2,1,0:T(8,128)(2,1)}), bf16[8,24,128]{2,1,0:T(8,128)(2,1)S(1)}, u32[]{:S(2)}, u32[]{:S(2)}) %all-to-all-start.1) | async-done | bytes 49184 | tf_op jit(solution)/shard_map/all_to_all | solution.py:19
  46.9 5.5 %all-to-all-start.2 = ((bf16[32,24,128]{2,1,0:T(8,128)(2,1)}), bf16[32,24,128]{2,1,0:T(8,128)(2,1)S(1)}, u32[]{:S(2)}, u32[]{:S(2)}) async-start(bf16[32,24,128]{2,1,0:T(8,128)(2,1)} %bitcast.14), calls=%async_computation.2 | async-start | bytes 393216 | tf_op jit(solution)/shard_map/all_to_all | solution.py:19
  52.4 8.4 %all-to-all-done.2 = bf16[32,24,128]{2,1,0:T(8,128)(2,1)S(1)} async-done(((bf16[32,24,128]{2,1,0:T(8,128)(2,1)}), bf16[32,24,128]{2,1,0:T(8,128)(2,1)S(1)}, u32[]{:S(2)}, u32[]{:S(2)}) %all-to-all-start.2) | async-done | bytes 196640 | tf_op jit(solution)/shard_map/all_to_all | solution.py:19
  61.1 24.3 %all_to_all.41 = bf16[16,16,512]{2,1,0:T(8,128)(2,1)S(1)} all-to-all(bf16[16,16,512]{2,1,0:T(8,128)(2,1)S(1)} %bitcast.81), channel_id=1, replica_groups=mesh['ep_0'=16,'ep_1'=4,'ep_2'=2,'tp'=4] {'ep_0'}, dimensions={0} | all-to-all | bytes 524288 | tf_op jit(solution)/shard_map/all_to_all | solution.py:19
  85.4 1.3 shard_map.205
  86.7 4.1 %all-to-all-start.4 = ((bf16[32,32,512]{2,1,0:T(8,128)(2,1)}), bf16[32,32,512]{2,1,0:T(8,128)(2,1)S(1)}, u32[]{:S(2)}, u32[]{:S(2)}) async-start(bf16[32,32,512]{2,1,0:T(8,128)(2,1)} %bitcast.19), calls=%async_computation.4 | async-start | bytes 2097152 | tf_op jit(solution)/shard_map/all_to_all | solution.py:19
  90.8 17.0 %all-to-all-done.4 = bf16[32,32,512]{2,1,0:T(8,128)(2,1)S(1)} async-done(((bf16[32,32,512]{2,1,0:T(8,128)(2,1)}), bf16[32,32,512]{2,1,0:T(8,128)(2,1)S(1)}, u32[]{:S(2)}, u32[]{:S(2)}) %all-to-all-start.4) | async-done | bytes 1048608 | tf_op jit(solution)/shard_map/all_to_all | solution.py:19
  107.8 2.9 %expert.1 = bf16[8,4,32,512]{3,2,1,0:T(8,128)(2,1)} custom-call(bf16[8,4,32,512]{3,2,1,0:T(8,128)(2,1)S(1)} %bitcast.71, bf16[1,2048]{1,0:T(2,128)(2,1)S(1)} %broadcast_in_dim.38.gain, bf16[2048,128]{1,0:T(8,128)(2,1)S(1)} %bitcast.78, bf16[2048,128]{1,0:T(8,128)(2,1)S(1)} %bitcast.79, bf16[128,2048]{1,0:T(8,128)(2,1)S(1)} %bitcast.80), custom_call_target="tpu_custom_call" | custom-call | tf_op jit(solution)/shard_map/expert/pallas_call | solution.py:151
  110.7 4.1 %all-to-all-start.5 = ((bf16[32,32,512]{2,1,0:T(8,128)(2,1)}), bf16[32,32,512]{2,1,0:T(8,128)(2,1)S(1)}, u32[]{:S(2)}, u32[]{:S(2)}) async-start(bf16[32,32,512]{2,1,0:T(8,128)(2,1)} %bitcast.24), calls=%async_computation.5 | async-start | bytes 2097152 | tf_op jit(solution)/shard_map/all_to_all | solution.py:19
  114.8 24.9 %all-gather = bf16[64,3,16,128]{3,2,1,0:T(8,128)(2,1)S(1)} all-gather(bf16[16,3,16,128]{3,2,1,0:T(8,128)(2,1)S(1)} %slice-done), channel_id=2, replica_groups=mesh['ep_0'=16,'ep_1'=4,'ep_2'=2,'tp'=4] {'ep_1'}, dimensions={0}, use_global_device_ids=true | all-gather | bytes 983040 | tf_op jit(solution)/shard_map/all_gather | solution.py:304
  139.9 1.9 %collective-permute-start.3 = (bf16[4,16,3,16,128]{4,3,0,1,2:T(8,128)(2,1)S(1)}, bf16[4,16,3,16,128]{4,3,0,1,2:T(8,128)(2,1)}, u32[]{:S(2)}, u32[]{:S(2)}) collective-permute-start(bf16[4,16,3,16,128]{4,3,0,1,2:T(8,128)(2,1)S(1)} %copy.54), channel_id=1, source_target_pairs={{0,4},{4,0},{1,5},{5,1},{2,6},{6,2},{3,7},{7,3},{8,12},{12,8},{9,1... | collective-permute-start | bytes 2359304 | tf_op jit(solution)/shard_map/ppermute | solution.py:305
  141.8 3.4 %collective-permute-start = (bf16[24,512]{1,0:T(8,128)(2,1)S(1)}, bf16[24,512]{1,0:T(8,128)(2,1)S(1)}, u32[]{:S(2)}, u32[]{:S(2)}) collective-permute-start(bf16[24,512]{1,0:T(8,128)(2,1)S(1)} %get-tuple-element.10), channel_id=1, source_target_pairs={{0,1},{1,2},{2,3},{3,0},{4,5},{5,6},{6,7},{7,4},{8,9},{9,10},{10,1... | collective-permute-start | bytes 73736 | tf_op jit(solution)/shard_map/ppermute | solution.py:30
  145.2 4.6 %collective-permute-start.1 = (bf16[24,512]{1,0:T(8,128)(2,1)S(1)}, bf16[24,512]{1,0:T(8,128)(2,1)S(1)}, u32[]{:S(2)}, u32[]{:S(2)}) collective-permute-start(bf16[24,512]{1,0:T(8,128)(2,1)S(1)} %get-tuple-element.10), channel_id=1, source_target_pairs={{0,2},{1,3},{2,0},{3,1},{4,6},{5,7},{6,4},{7,5},{8,10},{9,11},{10,... | collective-permute-start | bytes 73736 | tf_op jit(solution)/shard_map/ppermute | solution.py:30
  149.8 3.4 %collective-permute-start.2 = (bf16[24,512]{1,0:T(8,128)(2,1)S(1)}, bf16[24,512]{1,0:T(8,128)(2,1)S(1)}, u32[]{:S(2)}, u32[]{:S(2)}) collective-permute-start(bf16[24,512]{1,0:T(8,128)(2,1)S(1)} %get-tuple-element.10), channel_id=1, source_target_pairs={{0,3},{1,0},{2,1},{3,2},{4,7},{5,4},{6,5},{7,6},{8,11},{9,8},{10,9... | collective-permute-start | bytes 73736 | tf_op jit(solution)/shard_map/ppermute | solution.py:30
  154.1 1.4 collective-permute-done.2
  155.6 1.0 shard_map.206
  156.6 6.1 %all-to-all-start.6 = ((bf16[16,16,512]{2,1,0:T(8,128)(2,1)}), bf16[16,16,512]{2,1,0:T(8,128)(2,1)S(1)}, u32[]{:S(2)}, u32[]{:S(2)}) async-start(bf16[16,16,512]{2,1,0:T(8,128)(2,1)} %bitcast.26), calls=%async_computation.6 | async-start | bytes 524288 | tf_op jit(solution)/shard_map/all_to_all | solution.py:19
  162.7 1.2 select_bitcast_fusion.1
  165.1 1.9 %collective-permute-start.4 = (bf16[24,512]{1,0:T(8,128)(2,1)S(1)}, bf16[24,512]{1,0:T(8,128)(2,1)S(1)}, u32[]{:S(2)}, u32[]{:S(2)}) collective-permute-start(bf16[24,512]{1,0:T(8,128)(2,1)S(1)} %get-tuple-element.21), channel_id=1, source_target_pairs={{0,1},{1,2},{2,3},{3,0},{4,5},{5,6},{6,7},{7,4},{8,9},{9,10},{10,1... | collective-permute-start | bytes 73736 | tf_op jit(solution)/shard_map/ppermute | solution.py:30
  167.0 6.0 %collective-permute-start.5 = (bf16[24,512]{1,0:T(8,128)(2,1)S(1)}, bf16[24,512]{1,0:T(8,128)(2,1)S(1)}, u32[]{:S(2)}, u32[]{:S(2)}) collective-permute-start(bf16[24,512]{1,0:T(8,128)(2,1)S(1)} %get-tuple-element.23), channel_id=1, source_target_pairs={{0,2},{1,3},{2,0},{3,1},{4,6},{5,7},{6,4},{7,5},{8,10},{9,11},{10,... | collective-permute-start | bytes 73736 | tf_op jit(solution)/shard_map/ppermute | solution.py:30
  173.1 1.9 %collective-permute-start.6 = (bf16[24,512]{1,0:T(8,128)(2,1)S(1)}, bf16[24,512]{1,0:T(8,128)(2,1)S(1)}, u32[]{:S(2)}, u32[]{:S(2)}) collective-permute-start(bf16[24,512]{1,0:T(8,128)(2,1)S(1)} %get-tuple-element.22), channel_id=1, source_target_pairs={{0,3},{1,0},{2,1},{3,2},{4,7},{5,4},{6,5},{7,6},{8,11},{9,8},{10,9... | collective-permute-start | bytes 73736 | tf_op jit(solution)/shard_map/ppermute | solution.py:30
  175.2 3.7 %collective-permute-done.6 = bf16[24,512]{1,0:T(8,128)(2,1)S(1)} collective-permute-done((bf16[24,512]{1,0:T(8,128)(2,1)S(1)}, bf16[24,512]{1,0:T(8,128)(2,1)S(1)}, u32[]{:S(2)}, u32[]{:S(2)}) %collective-permute-start.6) | collective-permute-done | bytes 24608 | tf_op jit(solution)/shard_map/ppermute | solution.py:30
  178.8 1.7 all-to-all-done.6
  181.5 4.0 %all-to-all-start.7 = ((f32[4,1,24]{2,1,0:T(1,128)}), f32[4,1,24]{2,1,0:T(1,128)S(1)}, u32[]{:S(2)}, u32[]{:S(2)}) async-start(f32[4,1,24]{2,1,0:T(1,128)} %broadcast_in_dim.40), calls=%async_computation.7 | async-start | bytes 4096 | tf_op jit(solution)/shard_map/all_to_all | solution.py:19
  185.5 5.2 %all-to-all-done.7 = f32[4,1,24]{2,1,0:T(1,128)S(1)} async-done(((f32[4,1,24]{2,1,0:T(1,128)}), f32[4,1,24]{2,1,0:T(1,128)S(1)}, u32[]{:S(2)}, u32[]{:S(2)}) %all-to-all-start.7) | async-done | bytes 416 | tf_op jit(solution)/shard_map/all_to_all | solution.py:19
  (81 shorter events, 10.2 us)
Async XLA Ops:
  0.6 21.2 %copy-start = (bf16[2048,128]{1,0:T(8,128)(2,1)S(1)}, bf16[2048,128]{1,0:T(8,128)(2,1)}, u32[]{:S(2)}) copy-start(bf16[2048,128]{1,0:T(8,128)(2,1)} %param.23) | copy-start | bytes 1572868
  0.6 20.6 %copy-start.6 = (bf16[24,2048]{1,0:T(8,128)(2,1)S(1)}, bf16[24,2048]{1,0:T(8,128)(2,1)}, u32[]{:S(2)}) copy-start(bf16[24,2048]{1,0:T(8,128)(2,1)} %param.20) | copy-start | bytes 294916
  0.7 21.1 %copy-start.15 = (f32[1,128]{1,0:T(1,128)S(1)}, f32[1,128]{1,0:T(1,128)}, u32[]{:S(2)}) copy-start(f32[1,128]{1,0:T(1,128)} %param.25) | copy-start | bytes 1540
  0.7 20.6 %copy-start.8 = (bf16[2048,128]{1,0:T(8,128)(2,1)S(1)}, bf16[2048,128]{1,0:T(8,128)(2,1)}, u32[]{:S(2)}) copy-start(bf16[2048,128]{1,0:T(8,128)(2,1)} %param.22) | copy-start | bytes 1572868
  0.7 20.9 %copy-start.11 = (s32[24,6]{0,1:T(8,128)S(1)}, s32[24,6]{0,1:T(8,128)}, u32[]{:S(2)}) copy-start(s32[24,6]{0,1:T(8,128)} %param.35) | copy-start | bytes 1732
  0.7 21.4 %copy-start.7 = (f32[24,1,128,128]{3,2,1,0:T(8,128)S(1)}, f32[24,1,128,128]{3,2,1,0:T(8,128)}, u32[]{:S(2)}) copy-start(f32[24,1,128,128]{3,2,1,0:T(8,128)} %param.21) | copy-start | bytes 4718596
  2.3 33.1 %all-to-all-start = ((bf16[16,4,16,128]{3,2,1,0:T(8,128)(2,1)}), bf16[16,4,16,128]{3,2,1,0:T(8,128)(2,1)S(1)}, u32[]{:S(2)}, u32[]{:S(2)}) async-start(bf16[16,4,16,128]{3,2,1,0:T(8,128)(2,1)} %broadcast_in_dim.32), calls=%async_computation | async-start | bytes 524288 | tf_op jit(solution)/shard_map/all_to_all | solution.py:19
  23.1 1.6 copy-start.5
  23.1 1.6 copy-start.16
  35.5 55.3 %copy-start.1 = (bf16[16,4,16,128]{3,2,1,0:T(8,128)(2,1)}, bf16[16,4,16,128]{3,2,1,0:T(8,128)(2,1)S(1)}, u32[]{:S(2)}) copy-start(bf16[16,4,16,128]{3,2,1,0:T(8,128)(2,1)S(1)} %all-to-all-done.parts) | copy-start | bytes 786436
  36.1 9.8 %all-to-all-start.1 = ((bf16[8,24,128]{2,1,0:T(8,128)(2,1)}), bf16[8,24,128]{2,1,0:T(8,128)(2,1)S(1)}, u32[]{:S(2)}, u32[]{:S(2)}) async-start(bf16[8,24,128]{2,1,0:T(8,128)(2,1)} %broadcast_in_dim.33), calls=%async_computation.1 | async-start | bytes 98304 | tf_op jit(solution)/shard_map/all_to_all | solution.py:19
  46.9 13.9 %all-to-all-start.2 = ((bf16[32,24,128]{2,1,0:T(8,128)(2,1)}), bf16[32,24,128]{2,1,0:T(8,128)(2,1)S(1)}, u32[]{:S(2)}, u32[]{:S(2)}) async-start(bf16[32,24,128]{2,1,0:T(8,128)(2,1)} %bitcast.14), calls=%async_computation.2 | async-start | bytes 393216 | tf_op jit(solution)/shard_map/all_to_all | solution.py:19
  85.4 5.3 %copy-start.10 = (bf16[2048]{0:T(1024)(128)(2,1)S(1)}, bf16[2048]{0:T(1024)(128)(2,1)}, u32[]{:S(2)}) copy-start(bf16[2048]{0:T(1024)(128)(2,1)} %param.29) | copy-start | bytes 12292
  86.7 21.1 %copy-start.2 = (bf16[1,2048,128]{2,1,0:T(8,128)(2,1)S(1)}, bf16[1,2048,128]{2,1,0:T(8,128)(2,1)}, u32[]{:S(2)}) copy-start(bf16[1,2048,128]{2,1,0:T(8,128)(2,1)} %param.37) | copy-start | bytes 1572868
  86.7 21.1 %copy-start.3 = (bf16[1,2048,128]{2,1,0:T(8,128)(2,1)S(1)}, bf16[1,2048,128]{2,1,0:T(8,128)(2,1)}, u32[]{:S(2)}) copy-start(bf16[1,2048,128]{2,1,0:T(8,128)(2,1)} %param.38) | copy-start | bytes 1572868
  86.7 21.1 %copy-start.4 = (bf16[1,128,2048]{2,1,0:T(8,128)(2,1)S(1)}, bf16[1,128,2048]{2,1,0:T(8,128)(2,1)}, u32[]{:S(2)}) copy-start(bf16[1,128,2048]{2,1,0:T(8,128)(2,1)} %param.39) | copy-start | bytes 1572868
  86.7 21.1 %all-to-all-start.4 = ((bf16[32,32,512]{2,1,0:T(8,128)(2,1)}), bf16[32,32,512]{2,1,0:T(8,128)(2,1)S(1)}, u32[]{:S(2)}, u32[]{:S(2)}) async-start(bf16[32,32,512]{2,1,0:T(8,128)(2,1)} %bitcast.19), calls=%async_computation.4 | async-start | bytes 2097152 | tf_op jit(solution)/shard_map/all_to_all | solution.py:19
  110.7 4.1 %slice-start = ((bf16[16,4,16,128]{3,2,1,0:T(8,128)(2,1)}), bf16[16,3,16,128]{3,2,1,0:T(8,128)(2,1)S(1)}, s32[]{:S(2)}) async-start(bf16[16,4,16,128]{3,2,1,0:T(8,128)(2,1)} %copy-done.1), calls=%async_computation.8 | async-start | bytes 393216 | tf_op jit(solution)/shard_map/slice | solution.py:304
  110.7 44.9 %all-to-all-start.5 = ((bf16[32,32,512]{2,1,0:T(8,128)(2,1)}), bf16[32,32,512]{2,1,0:T(8,128)(2,1)S(1)}, u32[]{:S(2)}, u32[]{:S(2)}) async-start(bf16[32,32,512]{2,1,0:T(8,128)(2,1)} %bitcast.24), calls=%async_computation.5 | async-start | bytes 2097152 | tf_op jit(solution)/shard_map/all_to_all | solution.py:19
  114.8 38.4 %copy-start.12 = (f32[24,6]{0,1:T(8,128)S(1)}, f32[24,6]{0,1:T(8,128)}, u32[]{:S(2)}) copy-start(f32[24,6]{0,1:T(8,128)} %param.36) | copy-start | bytes 1732
  114.8 38.5 %copy-start.13 = (bf16[2048]{0:T(1024)(128)(2,1)S(1)}, bf16[2048]{0:T(1024)(128)(2,1)}, u32[]{:S(2)}) copy-start(bf16[2048]{0:T(1024)(128)(2,1)} %param.31) | copy-start | bytes 12292
  139.9 22.8 %collective-permute-start.3 = (bf16[4,16,3,16,128]{4,3,0,1,2:T(8,128)(2,1)S(1)}, bf16[4,16,3,16,128]{4,3,0,1,2:T(8,128)(2,1)}, u32[]{:S(2)}, u32[]{:S(2)}) collective-permute-start(bf16[4,16,3,16,128]{4,3,0,1,2:T(8,128)(2,1)S(1)} %copy.54), channel_id=1, source_target_pairs={{0,4},{4,0},{1,5},{5,1},{2,6},{6,2},{3,7},{7,3},{8,12},{12,8},{9,1... | collective-permute-start | bytes 2359304 | tf_op jit(solution)/shard_map/ppermute | solution.py:305
  141.8 12.3 %collective-permute-start = (bf16[24,512]{1,0:T(8,128)(2,1)S(1)}, bf16[24,512]{1,0:T(8,128)(2,1)S(1)}, u32[]{:S(2)}, u32[]{:S(2)}) collective-permute-start(bf16[24,512]{1,0:T(8,128)(2,1)S(1)} %get-tuple-element.10), channel_id=1, source_target_pairs={{0,1},{1,2},{2,3},{3,0},{4,5},{5,6},{6,7},{7,4},{8,9},{9,10},{10,1... | collective-permute-start | bytes 73736 | tf_op jit(solution)/shard_map/ppermute | solution.py:30
  145.2 8.9 %collective-permute-start.1 = (bf16[24,512]{1,0:T(8,128)(2,1)S(1)}, bf16[24,512]{1,0:T(8,128)(2,1)S(1)}, u32[]{:S(2)}, u32[]{:S(2)}) collective-permute-start(bf16[24,512]{1,0:T(8,128)(2,1)S(1)} %get-tuple-element.10), channel_id=1, source_target_pairs={{0,2},{1,3},{2,0},{3,1},{4,6},{5,7},{6,4},{7,5},{8,10},{9,11},{10,... | collective-permute-start | bytes 73736 | tf_op jit(solution)/shard_map/ppermute | solution.py:30
  149.8 5.7 %collective-permute-start.2 = (bf16[24,512]{1,0:T(8,128)(2,1)S(1)}, bf16[24,512]{1,0:T(8,128)(2,1)S(1)}, u32[]{:S(2)}, u32[]{:S(2)}) collective-permute-start(bf16[24,512]{1,0:T(8,128)(2,1)S(1)} %get-tuple-element.10), channel_id=1, source_target_pairs={{0,3},{1,0},{2,1},{3,2},{4,7},{5,4},{6,5},{7,6},{8,11},{9,8},{10,9... | collective-permute-start | bytes 73736 | tf_op jit(solution)/shard_map/ppermute | solution.py:30
  156.6 23.9 %all-to-all-start.6 = ((bf16[16,16,512]{2,1,0:T(8,128)(2,1)}), bf16[16,16,512]{2,1,0:T(8,128)(2,1)S(1)}, u32[]{:S(2)}, u32[]{:S(2)}) async-start(bf16[16,16,512]{2,1,0:T(8,128)(2,1)} %bitcast.26), calls=%async_computation.6 | async-start | bytes 524288 | tf_op jit(solution)/shard_map/all_to_all | solution.py:19
  164.5 16.0 %copy-start.9 = (f32[24,256]{0,1:T(8,128)S(1)}, f32[24,256]{0,1:T(8,128)}, u32[]{:S(2)}) copy-start(f32[24,256]{0,1:T(8,128)} %copy.52) | copy-start | bytes 73732
  164.5 21.0 %copy-start.14 = (bf16[512]{0:T(512)(128)(2,1)S(1)}, bf16[512]{0:T(512)(128)(2,1)}, u32[]{:S(2)}) copy-start(bf16[512]{0:T(512)(128)(2,1)} %param.30) | copy-start | bytes 3076
  165.1 10.0 %collective-permute-start.4 = (bf16[24,512]{1,0:T(8,128)(2,1)S(1)}, bf16[24,512]{1,0:T(8,128)(2,1)S(1)}, u32[]{:S(2)}, u32[]{:S(2)}) collective-permute-start(bf16[24,512]{1,0:T(8,128)(2,1)S(1)} %get-tuple-element.21), channel_id=1, source_target_pairs={{0,1},{1,2},{2,3},{3,0},{4,5},{5,6},{6,7},{7,4},{8,9},{9,10},{10,1... | collective-permute-start | bytes 73736 | tf_op jit(solution)/shard_map/ppermute | solution.py:30
  167.0 8.1 %collective-permute-start.5 = (bf16[24,512]{1,0:T(8,128)(2,1)S(1)}, bf16[24,512]{1,0:T(8,128)(2,1)S(1)}, u32[]{:S(2)}, u32[]{:S(2)}) collective-permute-start(bf16[24,512]{1,0:T(8,128)(2,1)S(1)} %get-tuple-element.23), channel_id=1, source_target_pairs={{0,2},{1,3},{2,0},{3,1},{4,6},{5,7},{6,4},{7,5},{8,10},{9,11},{10,... | collective-permute-start | bytes 73736 | tf_op jit(solution)/shard_map/ppermute | solution.py:30
  173.1 5.7 %collective-permute-start.6 = (bf16[24,512]{1,0:T(8,128)(2,1)S(1)}, bf16[24,512]{1,0:T(8,128)(2,1)S(1)}, u32[]{:S(2)}, u32[]{:S(2)}) collective-permute-start(bf16[24,512]{1,0:T(8,128)(2,1)S(1)} %get-tuple-element.22), channel_id=1, source_target_pairs={{0,3},{1,0},{2,1},{3,2},{4,7},{5,4},{6,5},{7,6},{8,11},{9,8},{10,9... | collective-permute-start | bytes 73736 | tf_op jit(solution)/shard_map/ppermute | solution.py:30
  181.5 9.2 %all-to-all-start.7 = ((f32[4,1,24]{2,1,0:T(1,128)}), f32[4,1,24]{2,1,0:T(1,128)S(1)}, u32[]{:S(2)}, u32[]{:S(2)}) async-start(f32[4,1,24]{2,1,0:T(1,128)} %broadcast_in_dim.40), calls=%async_computation.7 | async-start | bytes 4096 | tf_op jit(solution)/shard_map/all_to_all | solution.py:19

commit v3 on v2

--- a/solution.py
+++ b/solution.py
@@ -97,7 +97,21 @@
         out[:, t] = moved.reshape(cores, rows, width)
 
 
-def collect_body(terms, out):
+def combine_body(weights, returned, shared, mix, branch, squares):
+    rest = weights[...]
+    total = mix[:, :1] * shared[...].astype(F32)
+    for _ in range(3):
+        part = rest.astype(BF)
+        rest = rest - part.astype(F32)
+        total = total + jnp.dot(part, returned[...], preferred_element_type=F32)
+    branch[...] = total
+    square = jnp.sum(total * total, axis=1, keepdims=True)
+    squares[...] = jnp.broadcast_to(square[None], squares.shape)
+
+
+def collect_body(terms, first, second, third, fourth, out, shared):
+    parts = [r[...].astype(F32) for r in (first, second, third, fourth)]
+    shared[...] = (parts[0] + parts[1] + parts[2] + parts[3]).astype(BF)
     cores, n_tp, rows, width = terms.shape
     total = terms[:, 0].astype(F32)
     for t in range(1, n_tp):
@@ -120,7 +134,9 @@
         hn[:, cols] = (x[1](j).astype(F32) * scale * gain[:, cols].astype(F32)).astype(BF)
 
 
-def expert_body(x, gain, gate_hbm, up_hbm, down_hbm, out, hn, gate_w, up_w, down_w, sems):
+def expert_body(
+    x, gain, gate_hbm, up_hbm, down_hbm, out, hn, gate_w, up_w, down_w, held, sems, sent
+):
     cores, n_tp, rows, slice_width = x.shape
     total = cores * rows
     copies = [
@@ -141,7 +157,11 @@
     for j in range(n_tp):
         cols = pl.ds(j * slice_width, slice_width)
         part = jnp.dot(hidden, down_w[:, cols], preferred_element_type=F32).astype(BF)
-        out[:, j] = part.reshape(cores, rows, slice_width)
+        held[j] = part.reshape(cores, rows, slice_width)
+        copies.append(pltpu.make_async_copy(held.at[j], out.at[:, j], sent.at[j]))
+        copies[-1].start()
+    for copy in copies[3:]:
+        copy.wait()
 
 
 def expert_kernel(x, gain, gate_w, up_w, down_w):
@@ -152,13 +172,15 @@
         expert_body,
         out_shape=jax.ShapeDtypeStruct(x.shape, BF),
         in_specs=[vmem, vmem, hbm, hbm, hbm],
-        out_specs=vmem,
+        out_specs=hbm,
         scratch_shapes=[
             pltpu.VMEM((cores * rows, n_tp * slice_width), BF),
             pltpu.VMEM(gate_w.shape, BF),
             pltpu.VMEM(up_w.shape, BF),
             pltpu.VMEM(down_w.shape, BF),
+            pltpu.VMEM((n_tp, cores, rows, slice_width), BF),
             pltpu.SemaphoreType.DMA((3,)),
+            pltpu.SemaphoreType.DMA((n_tp,)),
         ],
         compiler_params=pltpu.CompilerParams(vmem_limit_bytes=32 * 1024 * 1024),
         name="expert",
@@ -253,7 +275,8 @@
     rank = jnp.dot(tri, named, preferred_element_type=F32)
     taken = (named > 0) & (rank == (column[0] % 2).astype(F32))
     chosen = jnp.where(taken, 1.0, 0.0).astype(BF).T
-    combine = jnp.where(taken, jnp.sum(jnp.where(hits, route_weights[:, :, None], 0.0), axis=1), 0.0)
+    combine = jnp.where(hits, route_weights[:, :, None], 0.0)
+    combine = jnp.where(taken, jnp.sum(combine, axis=1), 0.0)
     normed = rmsnorm(tokens.astype(F32), gain_mix).astype(BF)
     queries = jax.nn.silu(jnp.dot(normed, w_query, preferred_element_type=F32))
     forget_pre = jnp.dot(normed, w_forget, preferred_element_type=F32)
@@ -266,8 +289,9 @@
     new_state = forget[..., None] * carried_state + keys_in[..., None] * values_in[:, :, None, :]
     readout = jnp.einsum("bhd,bhdv->bhv", queries, new_state, precision=lax.Precision.HIGHEST)
     head_out = rmsnorm(readout, head_gain).astype(BF).reshape(seq_rows, head_dim)
-    head_out, parts = lax.optimization_barrier((head_out, parts))
-    heads = to_all(head_out, ("ep_1", "ep_2"))
+    heads = jnp.broadcast_to(head_out[None], (cores, seq_rows, head_dim))
+    heads, parts = lax.optimization_barrier((heads, parts))
+    heads = exchanged(heads, ("ep_1", "ep_2"))
     terms = vmem_call(
         project_body, jax.ShapeDtypeStruct((cores, n_tp, seq_rows, 128), BF), (heads, parts)
     )
@@ -294,13 +318,6 @@
     x = exchanged(spread.reshape(plane), ("ep_1", "ep_2", "tp")).reshape(spread.shape)
     down_terms = expert_kernel(x, gain_ffn[None], expert_gate[0], expert_up[0], expert_down[0])
     down_terms = exchanged(down_terms.reshape(plane), ("ep_1", "ep_2", "tp"))
-    summed = vmem_call(
-        collect_body,
-        jax.ShapeDtypeStruct((slots_all, slice_width), BF),
-        (down_terms.reshape(spread.shape),),
-    )
-    returned = exchanged(summed.reshape(n_z, 2 * cores, slice_width), "ep_0")
-    returned = returned.reshape(slots_all, slice_width)
     shared = lax.all_gather(parts[:, 1:], "ep_1")
     other = lax.ppermute(shared, "ep_2", [(0, 1), (1, 0)])
     first = lax.axis_index("ep_2") == 0
@@ -316,11 +333,25 @@
         shared[2],
     )
     shared_parts = [turned(shared_terms[k], k, n_tp) for k in range(n_tp)]
-    shared_out = sum(p.astype(F32) for p in shared_parts).astype(BF)
-    routed = jnp.dot(combine, returned.astype(F32), precision=lax.Precision.HIGHEST)
-    branch_sum = routed + mix[:, :1] * shared_out.astype(F32)
-    square_part = jnp.sum(branch_sum * branch_sum, axis=1)
-    square_total = jnp.sum(to_all(square_part, "tp"), axis=0)
+    summed, shared_out = vmem_call(
+        collect_body,
+        (
+            jax.ShapeDtypeStruct((slots_all, slice_width), BF),
+            jax.ShapeDtypeStruct((seq_rows, slice_width), BF),
+        ),
+        (down_terms.reshape(spread.shape), *shared_parts),
+    )
+    returned = exchanged(summed.reshape(n_z, 2 * cores, slice_width), "ep_0")
+    returned = returned.reshape(slots_all, slice_width)
+    branch_sum, squares = vmem_call(
+        combine_body,
+        (
+            jax.ShapeDtypeStruct((seq_rows, slice_width), F32),
+            jax.ShapeDtypeStruct((n_tp, seq_rows, 128), F32),
+        ),
+        (combine, returned, shared_out, mix),
+    )
+    square_total = jnp.sum(exchanged(squares, "tp")[:, :, 0], axis=0)
     norm_scale = lax.rsqrt(square_total / model_width + epsilon)
     layer_out = resid.astype(F32) + branch_sum * norm_scale[:, None] * gain_post.astype(F32)
     return (layer_out.astype(BF), new_state)

time: 192 us -> 190 us (0.990)
  the two profiles are of different devices: /device:TPU:32 before, /device:TPU:2 now
where the time goes in v3:
time: 190 us; the launch traced here: 189 us
  blocking collectives  70.7 us (37%)
  starting transfers between devices  66 us (35%)
  waiting for transfers between devices  30.1 us (16%)
  Pallas kernels  7.04 us (4%)
  other arithmetic  6.92 us (4%)
  matrix products  3.4 us (2%)
  local copies, waits for them, and re-layouts  3.21 us (2%)
    all_to_all x2, blocking collectives, exchanged(): return lax.all_to_all(value, axes, 0, 0, tiled=True)  48.3 us
    all_to_all x6, starting transfers between devices, exchanged(): return lax.all_to_all(value, axes, 0, 0, tiled=True)  41.5 us
    all_to_all x6, waiting for transfers between devices, exchanged(): return lax.all_to_all(value, axes, 0, 0, tiled=True)  27.6 us
    ppermute x6, starting transfers between devices, turned(): lax.ppermute(value, 'tp', [(k, (k + step) % devices) for k in range(devic...  22.6 us
    all_gather x1, blocking collectives, shards(): shared = lax.all_gather(parts[:, 1:], 'ep_1')  22.4 us
  transfers between devices with their start and end apart: 13, of which 5 were waited for; matrix products, arithmetic and copies ran while one was open for 5% of the time, Pallas kernels for 2%

profile of v3, /device:TPU:2, one launch (start us, length us, event | category | flops | bytes accessed | tf_op | source)
XLA Modules:
  0.0 188.6 jit_solution(6233437385505418124)
XLA Ops:
  0.7 0.9 pad_maximum_fusion.1
  2.3 15.2 %all-to-all-start = ((bf16[16,4,16,128]{3,2,1,0:T(8,128)(2,1)}), bf16[16,4,16,128]{3,2,1,0:T(8,128)(2,1)S(1)}, u32[]{:S(2)}, u32[]{:S(2)}) async-start(bf16[16,4,16,128]{3,2,1,0:T(8,128)(2,1)} %broadcast_in_dim.31), calls=%async_computation | async-start | bytes 524288 | tf_op jit(solution)/shard_map/all_to_all | solution.py:19
  18.2 1.0 fusion.3
  19.9 1.3 fusion.11
  21.9 1.0 multiply_add_fusion
  22.9 1.4 fusion
  24.8 11.1 %all-to-all-done.parts = bf16[16,4,16,128]{3,2,1,0:T(8,128)(2,1)S(1)} async-done(((bf16[16,4,16,128]{3,2,1,0:T(8,128)(2,1)}), bf16[16,4,16,128]{3,2,1,0:T(8,128)(2,1)S(1)}, u32[]{:S(2)}, u32[]{:S(2)}) %all-to-all-start) | async-done | bytes 262176 | tf_op jit(solution)/shard_map/all_to_all | solution.py:19
  36.5 4.8 %all-to-all-start.1 = ((bf16[8,24,128]{2,1,0:T(8,128)(2,1)}), bf16[8,24,128]{2,1,0:T(8,128)(2,1)S(1)}, u32[]{:S(2)}, u32[]{:S(2)}) async-start(bf16[8,24,128]{2,1,0:T(8,128)(2,1)} %broadcast_in_dim.30), calls=%async_computation.1 | async-start | bytes 98304 | tf_op jit(solution)/shard_map/all_to_all | solution.py:19
  41.4 4.1 %all-to-all-done.1.heads = bf16[8,24,128]{2,1,0:T(8,128)(2,1)S(1)} async-done(((bf16[8,24,128]{2,1,0:T(8,128)(2,1)}), bf16[8,24,128]{2,1,0:T(8,128)(2,1)S(1)}, u32[]{:S(2)}, u32[]{:S(2)}) %all-to-all-start.1) | async-done | bytes 49184 | tf_op jit(solution)/shard_map/all_to_all | solution.py:19
  45.5 0.9 shard_map.203
  46.4 6.7 %all-to-all-start.2 = ((bf16[32,24,128]{2,1,0:T(8,128)(2,1)}), bf16[32,24,128]{2,1,0:T(8,128)(2,1)S(1)}, u32[]{:S(2)}, u32[]{:S(2)}) async-start(bf16[32,24,128]{2,1,0:T(8,128)(2,1)} %bitcast.14), calls=%async_computation.2 | async-start | bytes 393216 | tf_op jit(solution)/shard_map/all_to_all | solution.py:19
  53.3 7.0 %all-to-all-done.2 = bf16[32,24,128]{2,1,0:T(8,128)(2,1)S(1)} async-done(((bf16[32,24,128]{2,1,0:T(8,128)(2,1)}), bf16[32,24,128]{2,1,0:T(8,128)(2,1)S(1)}, u32[]{:S(2)}, u32[]{:S(2)}) %all-to-all-start.2) | async-done | bytes 196640 | tf_op jit(solution)/shard_map/all_to_all | solution.py:19
  60.6 24.0 %all_to_all.40 = bf16[16,16,512]{2,1,0:T(8,128)(2,1)S(1)} all-to-all(bf16[16,16,512]{2,1,0:T(8,128)(2,1)S(1)} %bitcast.79), channel_id=1, replica_groups=mesh['ep_0'=16,'ep_1'=4,'ep_2'=2,'tp'=4] {'ep_0'}, dimensions={0} | all-to-all | bytes 524288 | tf_op jit(solution)/shard_map/all_to_all | solution.py:19
  84.7 1.2 shard_map.205
  85.9 5.0 %all-to-all-start.4 = ((bf16[32,32,512]{2,1,0:T(8,128)(2,1)}), bf16[32,32,512]{2,1,0:T(8,128)(2,1)S(1)}, u32[]{:S(2)}, u32[]{:S(2)}) async-start(bf16[32,32,512]{2,1,0:T(8,128)(2,1)} %bitcast.19), calls=%async_computation.4 | async-start | bytes 2097152 | tf_op jit(solution)/shard_map/all_to_all | solution.py:19
  91.0 22.4 %all-gather = bf16[64,3,16,128]{3,2,1,0:T(8,128)(2,1)S(1)} all-gather(bf16[16,3,16,128]{3,2,1,0:T(8,128)(2,1)S(1)} %slice.30), channel_id=2, replica_groups=mesh['ep_0'=16,'ep_1'=4,'ep_2'=2,'tp'=4] {'ep_1'}, dimensions={0}, use_global_device_ids=true | all-gather | bytes 983040 | tf_op jit(solution)/shard_map/all_gather | solution.py:321
  113.4 1.1 copy.38
  114.5 1.9 %collective-permute-start.3 = (bf16[4,16,3,16,128]{4,3,0,1,2:T(8,128)(2,1)}, bf16[4,16,3,16,128]{4,3,0,1,2:T(8,128)(2,1)}, u32[]{:S(2)}, u32[]{:S(2)}) collective-permute-start(bf16[4,16,3,16,128]{4,3,0,1,2:T(8,128)(2,1)} %copy.38), channel_id=1, source_target_pairs={{0,4},{4,0},{1,5},{5,1},{2,6},{6,2},{3,7},{7,3},{8,12},{12,8},{9,1... | collective-permute-start | bytes 2359304 | tf_op jit(solution)/shard_map/ppermute | solution.py:322
  116.5 3.3 %collective-permute-start = (bf16[24,512]{1,0:T(8,128)(2,1)S(1)}, bf16[24,512]{1,0:T(8,128)(2,1)S(1)}, u32[]{:S(2)}, u32[]{:S(2)}) collective-permute-start(bf16[24,512]{1,0:T(8,128)(2,1)S(1)} %get-tuple-element.14), channel_id=1, source_target_pairs={{0,1},{1,2},{2,3},{3,0},{4,5},{5,6},{6,7},{7,4},{8,9},{9,10},{10,1... | collective-permute-start | bytes 73736 | tf_op jit(solution)/shard_map/ppermute | solution.py:30
  119.8 4.4 %collective-permute-start.1 = (bf16[24,512]{1,0:T(8,128)(2,1)S(1)}, bf16[24,512]{1,0:T(8,128)(2,1)S(1)}, u32[]{:S(2)}, u32[]{:S(2)}) collective-permute-start(bf16[24,512]{1,0:T(8,128)(2,1)S(1)} %get-tuple-element.14), channel_id=1, source_target_pairs={{0,2},{1,3},{2,0},{3,1},{4,6},{5,7},{6,4},{7,5},{8,10},{9,11},{10,... | collective-permute-start | bytes 73736 | tf_op jit(solution)/shard_map/ppermute | solution.py:30
  124.2 3.6 %collective-permute-start.2 = (bf16[24,512]{1,0:T(8,128)(2,1)S(1)}, bf16[24,512]{1,0:T(8,128)(2,1)S(1)}, u32[]{:S(2)}, u32[]{:S(2)}) collective-permute-start(bf16[24,512]{1,0:T(8,128)(2,1)S(1)} %get-tuple-element.14), channel_id=1, source_target_pairs={{0,3},{1,0},{2,1},{3,2},{4,7},{5,4},{6,5},{7,6},{8,11},{9,8},{10,9... | collective-permute-start | bytes 73736 | tf_op jit(solution)/shard_map/ppermute | solution.py:30
  127.9 2.7 %expert.1 = bf16[8,4,32,512]{3,2,1,0:T(8,128)(2,1)} custom-call(bf16[8,4,32,512]{3,2,1,0:T(8,128)(2,1)S(1)} %bitcast.67, bf16[1,2048]{1,0:T(2,128)(2,1)S(1)} %broadcast_in_dim.58.gain, bf16[2048,128]{1,0:T(8,128)(2,1)S(1)} %bitcast.75, bf16[2048,128]{1,0:T(8,128)(2,1)S(1)} %bitcast.76, bf16[128,2048]{1,0:T(8,128)(2,1)S(1)} %bitcast.77), custom_call_target="tpu_custom_call" | custom-call | tf_op jit(solution)/shard_map/expert/pallas_call | solution.py:171
  130.6 6.5 %all-to-all-start.5 = ((bf16[32,32,512]{2,1,0:T(8,128)(2,1)}), bf16[32,32,512]{2,1,0:T(8,128)(2,1)S(1)}, u32[]{:S(2)}, u32[]{:S(2)}) async-start(bf16[32,32,512]{2,1,0:T(8,128)(2,1)} %bitcast.24), calls=%async_computation.5 | async-start | bytes 2097152 | tf_op jit(solution)/shard_map/all_to_all | solution.py:19
  137.2 1.2 select_bitcast_fusion.1
  139.6 3.4 %collective-permute-start.4 = (bf16[24,512]{1,0:T(8,128)(2,1)S(1)}, bf16[24,512]{1,0:T(8,128)(2,1)S(1)}, u32[]{:S(2)}, u32[]{:S(2)}) collective-permute-start(bf16[24,512]{1,0:T(8,128)(2,1)S(1)} %get-tuple-element.29), channel_id=1, source_target_pairs={{0,1},{1,2},{2,3},{3,0},{4,5},{5,6},{6,7},{7,4},{8,9},{9,10},{10,1... | collective-permute-start | bytes 73736 | tf_op jit(solution)/shard_map/ppermute | solution.py:30
  143.0 4.6 %collective-permute-start.5 = (bf16[24,512]{1,0:T(8,128)(2,1)S(1)}, bf16[24,512]{1,0:T(8,128)(2,1)S(1)}, u32[]{:S(2)}, u32[]{:S(2)}) collective-permute-start(bf16[24,512]{1,0:T(8,128)(2,1)S(1)} %get-tuple-element.28), channel_id=1, source_target_pairs={{0,2},{1,3},{2,0},{3,1},{4,6},{5,7},{6,4},{7,5},{8,10},{9,11},{10,... | collective-permute-start | bytes 73736 | tf_op jit(solution)/shard_map/ppermute | solution.py:30
  147.6 3.4 %collective-permute-start.6 = (bf16[24,512]{1,0:T(8,128)(2,1)S(1)}, bf16[24,512]{1,0:T(8,128)(2,1)S(1)}, u32[]{:S(2)}, u32[]{:S(2)}) collective-permute-start(bf16[24,512]{1,0:T(8,128)(2,1)S(1)} %get-tuple-element.27), channel_id=1, source_target_pairs={{0,3},{1,0},{2,1},{3,2},{4,7},{5,4},{6,5},{7,6},{8,11},{9,8},{10,9... | collective-permute-start | bytes 73736 | tf_op jit(solution)/shard_map/ppermute | solution.py:30
  151.0 2.5 %collective-permute-done.4.second = bf16[24,512]{1,0:T(8,128)(2,1)S(1)} collective-permute-done((bf16[24,512]{1,0:T(8,128)(2,1)S(1)}, bf16[24,512]{1,0:T(8,128)(2,1)S(1)}, u32[]{:S(2)}, u32[]{:S(2)}) %collective-permute-start.4) | collective-permute-done | bytes 24608 | tf_op jit(solution)/shard_map/ppermute | solution.py:30
  153.8 24.2 %all_to_all.41 = bf16[16,16,512]{2,1,0:T(8,128)(2,1)S(1)} all-to-all(bf16[16,16,512]{2,1,0:T(8,128)(2,1)S(1)} %bitcast.78), channel_id=1, replica_groups=mesh['ep_0'=16,'ep_1'=4,'ep_2'=2,'tp'=4] {'ep_0'}, dimensions={0} | all-to-all | bytes 524288 | tf_op jit(solution)/shard_map/all_to_all | solution.py:19
  178.1 0.9 shard_map.207
  179.0 3.3 %all-to-all-start.7 = ((f32[4,24,128]{2,1,0:T(8,128)}), f32[4,24,128]{2,1,0:T(8,128)S(1)}, u32[]{:S(2)}, u32[]{:S(2)}) async-start(f32[4,24,128]{2,1,0:T(8,128)} %get-tuple-element.21), calls=%async_computation.7 | async-start | bytes 98304 | tf_op jit(solution)/shard_map/all_to_all | solution.py:19
  182.3 5.5 %all-to-all-done.7 = f32[4,24,128]{2,1,0:T(8,128)S(1)} async-done(((f32[4,24,128]{2,1,0:T(8,128)}), f32[4,24,128]{2,1,0:T(8,128)S(1)}, u32[]{:S(2)}, u32[]{:S(2)}) %all-to-all-start.7) | async-done | bytes 49184 | tf_op jit(solution)/shard_map/all_to_all | solution.py:19
  (75 shorter events, 6.7 us)
Async XLA Ops:
  0.6 20.9 %copy-start = (bf16[2048,128]{1,0:T(8,128)(2,1)S(1)}, bf16[2048,128]{1,0:T(8,128)(2,1)}, u32[]{:S(2)}) copy-start(bf16[2048,128]{1,0:T(8,128)(2,1)} %param.23) | copy-start | bytes 1572868
  0.6 20.6 %copy-start.7 = (bf16[24,2048]{1,0:T(8,128)(2,1)S(1)}, bf16[24,2048]{1,0:T(8,128)(2,1)}, u32[]{:S(2)}) copy-start(bf16[24,2048]{1,0:T(8,128)(2,1)} %param.20) | copy-start | bytes 294916
  0.7 20.9 %copy-start.15 = (f32[1,128]{1,0:T(1,128)S(1)}, f32[1,128]{1,0:T(1,128)}, u32[]{:S(2)}) copy-start(f32[1,128]{1,0:T(1,128)} %param.25) | copy-start | bytes 1540
  0.7 20.6 %copy-start.9 = (bf16[2048,128]{1,0:T(8,128)(2,1)S(1)}, bf16[2048,128]{1,0:T(8,128)(2,1)}, u32[]{:S(2)}) copy-start(bf16[2048,128]{1,0:T(8,128)(2,1)} %param.22) | copy-start | bytes 1572868
  0.7 21.2 %copy-start.8 = (f32[24,1,128,128]{3,2,1,0:T(8,128)S(1)}, f32[24,1,128,128]{3,2,1,0:T(8,128)}, u32[]{:S(2)}) copy-start(f32[24,1,128,128]{3,2,1,0:T(8,128)} %param.21) | copy-start | bytes 4718596
  2.3 33.6 %all-to-all-start = ((bf16[16,4,16,128]{3,2,1,0:T(8,128)(2,1)}), bf16[16,4,16,128]{3,2,1,0:T(8,128)(2,1)S(1)}, u32[]{:S(2)}, u32[]{:S(2)}) async-start(bf16[16,4,16,128]{3,2,1,0:T(8,128)(2,1)} %broadcast_in_dim.31), calls=%async_computation | async-start | bytes 524288 | tf_op jit(solution)/shard_map/all_to_all | solution.py:19
  22.9 1.9 copy-start.6
  22.9 1.6 copy-start.11
  22.9 1.7 copy-start.12
  22.9 1.8 copy-start.16
  36.5 8.9 %all-to-all-start.1 = ((bf16[8,24,128]{2,1,0:T(8,128)(2,1)}), bf16[8,24,128]{2,1,0:T(8,128)(2,1)S(1)}, u32[]{:S(2)}, u32[]{:S(2)}) async-start(bf16[8,24,128]{2,1,0:T(8,128)(2,1)} %broadcast_in_dim.30), calls=%async_computation.1 | async-start | bytes 98304 | tf_op jit(solution)/shard_map/all_to_all | solution.py:19
  46.4 13.9 %all-to-all-start.2 = ((bf16[32,24,128]{2,1,0:T(8,128)(2,1)}), bf16[32,24,128]{2,1,0:T(8,128)(2,1)S(1)}, u32[]{:S(2)}, u32[]{:S(2)}) async-start(bf16[32,24,128]{2,1,0:T(8,128)(2,1)} %bitcast.14), calls=%async_computation.2 | async-start | bytes 393216 | tf_op jit(solution)/shard_map/all_to_all | solution.py:19
  85.9 41.9 %all-to-all-start.4 = ((bf16[32,32,512]{2,1,0:T(8,128)(2,1)}), bf16[32,32,512]{2,1,0:T(8,128)(2,1)S(1)}, u32[]{:S(2)}, u32[]{:S(2)}) async-start(bf16[32,32,512]{2,1,0:T(8,128)(2,1)} %bitcast.19), calls=%async_computation.4 | async-start | bytes 2097152 | tf_op jit(solution)/shard_map/all_to_all | solution.py:19
  90.9 36.9 %copy-start.10 = (bf16[2048]{0:T(1024)(128)(2,1)S(1)}, bf16[2048]{0:T(1024)(128)(2,1)}, u32[]{:S(2)}) copy-start(bf16[2048]{0:T(1024)(128)(2,1)} %param.29) | copy-start | bytes 12292
  90.9 36.9 %copy-start.13 = (bf16[2048]{0:T(1024)(128)(2,1)S(1)}, bf16[2048]{0:T(1024)(128)(2,1)}, u32[]{:S(2)}) copy-start(bf16[2048]{0:T(1024)(128)(2,1)} %param.31) | copy-start | bytes 12292
  90.9 36.9 %copy-start.1 = (bf16[1,2048,128]{2,1,0:T(8,128)(2,1)S(1)}, bf16[1,2048,128]{2,1,0:T(8,128)(2,1)}, u32[]{:S(2)}) copy-start(bf16[1,2048,128]{2,1,0:T(8,128)(2,1)} %param.37) | copy-start | bytes 1572868
  90.9 36.9 %copy-start.2 = (bf16[1,2048,128]{2,1,0:T(8,128)(2,1)S(1)}, bf16[1,2048,128]{2,1,0:T(8,128)(2,1)}, u32[]{:S(2)}) copy-start(bf16[1,2048,128]{2,1,0:T(8,128)(2,1)} %param.38) | copy-start | bytes 1572868
  90.9 36.9 %copy-start.3 = (bf16[1,128,2048]{2,1,0:T(8,128)(2,1)S(1)}, bf16[1,128,2048]{2,1,0:T(8,128)(2,1)}, u32[]{:S(2)}) copy-start(bf16[1,128,2048]{2,1,0:T(8,128)(2,1)} %param.39) | copy-start | bytes 1572868
  113.4 10.7 %copy-start.4 = (bf16[64,3,16,128]{3,2,1,0:T(8,128)(2,1)}, bf16[64,3,16,128]{3,2,1,0:T(8,128)(2,1)S(1)}, u32[]{:S(2)}) copy-start(bf16[64,3,16,128]{3,2,1,0:T(8,128)(2,1)S(1)} %all-gather) | copy-start | bytes 2359300
  114.5 22.6 %collective-permute-start.3 = (bf16[4,16,3,16,128]{4,3,0,1,2:T(8,128)(2,1)}, bf16[4,16,3,16,128]{4,3,0,1,2:T(8,128)(2,1)}, u32[]{:S(2)}, u32[]{:S(2)}) collective-permute-start(bf16[4,16,3,16,128]{4,3,0,1,2:T(8,128)(2,1)} %copy.38), channel_id=1, source_target_pairs={{0,4},{4,0},{1,5},{5,1},{2,6},{6,2},{3,7},{7,3},{8,12},{12,8},{9,1... | collective-permute-start | bytes 2359304 | tf_op jit(solution)/shard_map/ppermute | solution.py:322
  116.5 20.7 %collective-permute-start = (bf16[24,512]{1,0:T(8,128)(2,1)S(1)}, bf16[24,512]{1,0:T(8,128)(2,1)S(1)}, u32[]{:S(2)}, u32[]{:S(2)}) collective-permute-start(bf16[24,512]{1,0:T(8,128)(2,1)S(1)} %get-tuple-element.14), channel_id=1, source_target_pairs={{0,1},{1,2},{2,3},{3,0},{4,5},{5,6},{6,7},{7,4},{8,9},{9,10},{10,1... | collective-permute-start | bytes 73736 | tf_op jit(solution)/shard_map/ppermute | solution.py:30
  119.8 17.4 %collective-permute-start.1 = (bf16[24,512]{1,0:T(8,128)(2,1)S(1)}, bf16[24,512]{1,0:T(8,128)(2,1)S(1)}, u32[]{:S(2)}, u32[]{:S(2)}) collective-permute-start(bf16[24,512]{1,0:T(8,128)(2,1)S(1)} %get-tuple-element.14), channel_id=1, source_target_pairs={{0,2},{1,3},{2,0},{3,1},{4,6},{5,7},{6,4},{7,5},{8,10},{9,11},{10,... | collective-permute-start | bytes 73736 | tf_op jit(solution)/shard_map/ppermute | solution.py:30
  124.2 13.0 %collective-permute-start.2 = (bf16[24,512]{1,0:T(8,128)(2,1)S(1)}, bf16[24,512]{1,0:T(8,128)(2,1)S(1)}, u32[]{:S(2)}, u32[]{:S(2)}) collective-permute-start(bf16[24,512]{1,0:T(8,128)(2,1)S(1)} %get-tuple-element.14), channel_id=1, source_target_pairs={{0,3},{1,0},{2,1},{3,2},{4,7},{5,4},{6,5},{7,6},{8,11},{9,8},{10,9... | collective-permute-start | bytes 73736 | tf_op jit(solution)/shard_map/ppermute | solution.py:30
  130.6 6.6 %copy-start.5 = (bf16[64,3,16,128]{3,2,1,0:T(8,128)(2,1)S(1)}, bf16[64,3,16,128]{3,2,1,0:T(8,128)(2,1)}, u32[]{:S(2)}) copy-start(bf16[64,3,16,128]{3,2,1,0:T(8,128)(2,1)} %copy-done.4) | copy-start | bytes 2359300
  130.6 22.9 %all-to-all-start.5 = ((bf16[32,32,512]{2,1,0:T(8,128)(2,1)}), bf16[32,32,512]{2,1,0:T(8,128)(2,1)S(1)}, u32[]{:S(2)}, u32[]{:S(2)}) async-start(bf16[32,32,512]{2,1,0:T(8,128)(2,1)} %bitcast.24), calls=%async_computation.5 | async-start | bytes 2097152 | tf_op jit(solution)/shard_map/all_to_all | solution.py:19
  139.6 42.7 %copy-start.14 = (bf16[512]{0:T(512)(128)(2,1)S(1)}, bf16[512]{0:T(512)(128)(2,1)}, u32[]{:S(2)}) copy-start(bf16[512]{0:T(512)(128)(2,1)} %param.30) | copy-start | bytes 3076
  139.6 13.9 %collective-permute-start.4 = (bf16[24,512]{1,0:T(8,128)(2,1)S(1)}, bf16[24,512]{1,0:T(8,128)(2,1)S(1)}, u32[]{:S(2)}, u32[]{:S(2)}) collective-permute-start(bf16[24,512]{1,0:T(8,128)(2,1)S(1)} %get-tuple-element.29), channel_id=1, source_target_pairs={{0,1},{1,2},{2,3},{3,0},{4,5},{5,6},{6,7},{7,4},{8,9},{9,10},{10,1... | collective-permute-start | bytes 73736 | tf_op jit(solution)/shard_map/ppermute | solution.py:30
  143.0 10.5 %collective-permute-start.5 = (bf16[24,512]{1,0:T(8,128)(2,1)S(1)}, bf16[24,512]{1,0:T(8,128)(2,1)S(1)}, u32[]{:S(2)}, u32[]{:S(2)}) collective-permute-start(bf16[24,512]{1,0:T(8,128)(2,1)S(1)} %get-tuple-element.28), channel_id=1, source_target_pairs={{0,2},{1,3},{2,0},{3,1},{4,6},{5,7},{6,4},{7,5},{8,10},{9,11},{10,... | collective-permute-start | bytes 73736 | tf_op jit(solution)/shard_map/ppermute | solution.py:30
  147.6 5.9 %collective-permute-start.6 = (bf16[24,512]{1,0:T(8,128)(2,1)S(1)}, bf16[24,512]{1,0:T(8,128)(2,1)S(1)}, u32[]{:S(2)}, u32[]{:S(2)}) collective-permute-start(bf16[24,512]{1,0:T(8,128)(2,1)S(1)} %get-tuple-element.27), channel_id=1, source_target_pairs={{0,3},{1,0},{2,1},{3,2},{4,7},{5,4},{6,5},{7,6},{8,11},{9,8},{10,9... | collective-permute-start | bytes 73736 | tf_op jit(solution)/shard_map/ppermute | solution.py:30
  179.0 8.8 %all-to-all-start.7 = ((f32[4,24,128]{2,1,0:T(8,128)}), f32[4,24,128]{2,1,0:T(8,128)S(1)}, u32[]{:S(2)}, u32[]{:S(2)}) async-start(f32[4,24,128]{2,1,0:T(8,128)} %get-tuple-element.21), calls=%async_computation.7 | async-start | bytes 98304 | tf_op jit(solution)/shard_map/all_to_all | solution.py:19

commit v4 on v3

--- a/solution.py
+++ b/solution.py
@@ -106,7 +106,23 @@
         total = total + jnp.dot(part, returned[...], preferred_element_type=F32)
     branch[...] = total
     square = jnp.sum(total * total, axis=1, keepdims=True)
-    squares[...] = jnp.broadcast_to(square[None], squares.shape)
+    group = lax.broadcasted_iota(jnp.int32, squares.shape[1:], 1)
+    packed = jnp.zeros(squares.shape[1:], F32)
+    for g in range(total.shape[0] // 8):
+        packed = jnp.where(group == g, square[8 * g : 8 * g + 8], packed)
+    squares[...] = jnp.broadcast_to(packed[None], squares.shape)
+
+
+def final_body(squares, branch, resid, gain, out):
+    n_tp = squares.shape[0]
+    total = squares[0]
+    for t in range(1, n_tp):
+        total = total + squares[t]
+    scale = lax.rsqrt(total / (n_tp * out.shape[1]) + epsilon)
+    for g in range(out.shape[0] // 8):
+        rows = pl.ds(8 * g, 8)
+        grown = branch[rows, :] * scale[:, g : g + 1] * gain[...]
+        out[rows, :] = (resid[rows, :].astype(F32) + grown).astype(BF)
 
 
 def collect_body(terms, first, second, third, fourth, out, shared):
@@ -347,14 +363,16 @@
         combine_body,
         (
             jax.ShapeDtypeStruct((seq_rows, slice_width), F32),
-            jax.ShapeDtypeStruct((n_tp, seq_rows, 128), F32),
+            jax.ShapeDtypeStruct((n_tp, 8, 128), F32),
         ),
         (combine, returned, shared_out, mix),
     )
-    square_total = jnp.sum(exchanged(squares, "tp")[:, :, 0], axis=0)
-    norm_scale = lax.rsqrt(square_total / model_width + epsilon)
-    layer_out = resid.astype(F32) + branch_sum * norm_scale[:, None] * gain_post.astype(F32)
-    return (layer_out.astype(BF), new_state)
+    layer_out = vmem_call(
+        final_body,
+        jax.ShapeDtypeStruct((seq_rows, slice_width), BF),
+        (exchanged(squares, "tp"), branch_sum, resid, gain_post.astype(F32)[None]),
+    )
+    return (layer_out, new_state)
 
 
 def solution(mesh):

time: 190 us -> 189 us (level)
    pallas_call x5 -> x6, Pallas kernels: 3.75 us -> 4.41 us  [vmem_call(): pl.pallas_call(body, out_shape=out_shape, in_specs=[vmem] * len(args), ou...]
where the time goes in v4:
time: 189 us; the launch traced here: 188 us
  blocking collectives  70.7 us (37%)
  starting transfers between devices  66 us (35%)
  waiting for transfers between devices  29.9 us (16%)
  Pallas kernels  7.67 us (4%)
  other arithmetic  6.1 us (3%)
  matrix products  3.4 us (2%)
  local copies, waits for them, and re-layouts  3.2 us (2%)
    all_to_all x2, blocking collectives, exchanged(): return lax.all_to_all(value, axes, 0, 0, tiled=True)  48.3 us
    all_to_all x6, starting transfers between devices, exchanged(): return lax.all_to_all(value, axes, 0, 0, tiled=True)  41.5 us
    all_to_all x6, waiting for transfers between devices, exchanged(): return lax.all_to_all(value, axes, 0, 0, tiled=True)  27.4 us
    ppermute x6, starting transfers between devices, turned(): lax.ppermute(value, 'tp', [(k, (k + step) % devices) for k in range(devic...  22.6 us
    all_gather x1, blocking collectives, shards(): shared = lax.all_gather(parts[:, 1:], 'ep_1')  22.4 us
    pallas_call x6, Pallas kernels, vmem_call(): pl.pallas_call(body, out_shape=out_shape, in_specs=[vmem] * len(args), ou...  4.41 us
  transfers between devices with their start and end apart: 13, of which 5 were waited for; matrix products, arithmetic and copies ran while one was open for 5% of the time, Pallas kernels for 2%

profile of v4, /device:TPU:2, one launch (start us, length us, event | category | flops | bytes accessed | tf_op | source)
XLA Modules:
  0.0 188.2 jit_solution(2775879453498031354)
XLA Ops:
  0.7 0.9 pad_maximum_fusion.1
  2.3 15.2 %all-to-all-start = ((bf16[16,4,16,128]{3,2,1,0:T(8,128)(2,1)}), bf16[16,4,16,128]{3,2,1,0:T(8,128)(2,1)S(1)}, u32[]{:S(2)}, u32[]{:S(2)}) async-start(bf16[16,4,16,128]{3,2,1,0:T(8,128)(2,1)} %broadcast_in_dim.59), calls=%async_computation | async-start | bytes 524288 | tf_op jit(solution)/shard_map/all_to_all | solution.py:19
  18.2 1.0 fusion.3
  19.9 1.3 fusion.11
  21.8 1.0 multiply_add_fusion
  22.9 1.4 fusion
  24.8 11.1 %all-to-all-done.parts = bf16[16,4,16,128]{3,2,1,0:T(8,128)(2,1)S(1)} async-done(((bf16[16,4,16,128]{3,2,1,0:T(8,128)(2,1)}), bf16[16,4,16,128]{3,2,1,0:T(8,128)(2,1)S(1)}, u32[]{:S(2)}, u32[]{:S(2)}) %all-to-all-start) | async-done | bytes 262176 | tf_op jit(solution)/shard_map/all_to_all | solution.py:19
  36.5 4.8 %all-to-all-start.1 = ((bf16[8,24,128]{2,1,0:T(8,128)(2,1)}), bf16[8,24,128]{2,1,0:T(8,128)(2,1)S(1)}, u32[]{:S(2)}, u32[]{:S(2)}) async-start(bf16[8,24,128]{2,1,0:T(8,128)(2,1)} %broadcast_in_dim.58), calls=%async_computation.1 | async-start | bytes 98304 | tf_op jit(solution)/shard_map/all_to_all | solution.py:19
  41.4 4.1 %all-to-all-done.1.heads = bf16[8,24,128]{2,1,0:T(8,128)(2,1)S(1)} async-done(((bf16[8,24,128]{2,1,0:T(8,128)(2,1)}), bf16[8,24,128]{2,1,0:T(8,128)(2,1)S(1)}, u32[]{:S(2)}, u32[]{:S(2)}) %all-to-all-start.1) | async-done | bytes 49184 | tf_op jit(solution)/shard_map/all_to_all | solution.py:19
  45.4 0.9 shard_map.203
  46.3 6.7 %all-to-all-start.2 = ((bf16[32,24,128]{2,1,0:T(8,128)(2,1)}), bf16[32,24,128]{2,1,0:T(8,128)(2,1)S(1)}, u32[]{:S(2)}, u32[]{:S(2)}) async-start(bf16[32,24,128]{2,1,0:T(8,128)(2,1)} %bitcast.14), calls=%async_computation.2 | async-start | bytes 393216 | tf_op jit(solution)/shard_map/all_to_all | solution.py:19
  53.3 7.0 %all-to-all-done.2 = bf16[32,24,128]{2,1,0:T(8,128)(2,1)S(1)} async-done(((bf16[32,24,128]{2,1,0:T(8,128)(2,1)}), bf16[32,24,128]{2,1,0:T(8,128)(2,1)S(1)}, u32[]{:S(2)}, u32[]{:S(2)}) %all-to-all-start.2) | async-done | bytes 196640 | tf_op jit(solution)/shard_map/all_to_all | solution.py:19
  60.6 24.0 %all_to_all.40 = bf16[16,16,512]{2,1,0:T(8,128)(2,1)S(1)} all-to-all(bf16[16,16,512]{2,1,0:T(8,128)(2,1)S(1)} %bitcast.80), channel_id=1, replica_groups=mesh['ep_0'=16,'ep_1'=4,'ep_2'=2,'tp'=4] {'ep_0'}, dimensions={0} | all-to-all | bytes 524288 | tf_op jit(solution)/shard_map/all_to_all | solution.py:19
  84.6 1.2 shard_map.205
  85.9 5.0 %all-to-all-start.4 = ((bf16[32,32,512]{2,1,0:T(8,128)(2,1)}), bf16[32,32,512]{2,1,0:T(8,128)(2,1)S(1)}, u32[]{:S(2)}, u32[]{:S(2)}) async-start(bf16[32,32,512]{2,1,0:T(8,128)(2,1)} %bitcast.19), calls=%async_computation.4 | async-start | bytes 2097152 | tf_op jit(solution)/shard_map/all_to_all | solution.py:19
  90.9 22.4 %all-gather = bf16[64,3,16,128]{3,2,1,0:T(8,128)(2,1)S(1)} all-gather(bf16[16,3,16,128]{3,2,1,0:T(8,128)(2,1)S(1)} %slice.27), channel_id=2, replica_groups=mesh['ep_0'=16,'ep_1'=4,'ep_2'=2,'tp'=4] {'ep_1'}, dimensions={0}, use_global_device_ids=true | all-gather | bytes 983040 | tf_op jit(solution)/shard_map/all_gather | solution.py:337
  113.4 1.1 copy.38
  114.5 1.9 %collective-permute-start.3 = (bf16[4,16,3,16,128]{4,3,0,1,2:T(8,128)(2,1)}, bf16[4,16,3,16,128]{4,3,0,1,2:T(8,128)(2,1)}, u32[]{:S(2)}, u32[]{:S(2)}) collective-permute-start(bf16[4,16,3,16,128]{4,3,0,1,2:T(8,128)(2,1)} %copy.38), channel_id=1, source_target_pairs={{0,4},{4,0},{1,5},{5,1},{2,6},{6,2},{3,7},{7,3},{8,12},{12,8},{9,1... | collective-permute-start | bytes 2359304 | tf_op jit(solution)/shard_map/ppermute | solution.py:338
  116.4 3.3 %collective-permute-start = (bf16[24,512]{1,0:T(8,128)(2,1)S(1)}, bf16[24,512]{1,0:T(8,128)(2,1)S(1)}, u32[]{:S(2)}, u32[]{:S(2)}) collective-permute-start(bf16[24,512]{1,0:T(8,128)(2,1)S(1)} %get-tuple-element.15.resid), channel_id=1, source_target_pairs={{0,1},{1,2},{2,3},{3,0},{4,5},{5,6},{6,7},{7,4},{8,9},{9,10},{10,1... | collective-permute-start | bytes 73736 | tf_op jit(solution)/shard_map/ppermute | solution.py:30
  119.7 4.4 %collective-permute-start.1 = (bf16[24,512]{1,0:T(8,128)(2,1)S(1)}, bf16[24,512]{1,0:T(8,128)(2,1)S(1)}, u32[]{:S(2)}, u32[]{:S(2)}) collective-permute-start(bf16[24,512]{1,0:T(8,128)(2,1)S(1)} %get-tuple-element.15.resid), channel_id=1, source_target_pairs={{0,2},{1,3},{2,0},{3,1},{4,6},{5,7},{6,4},{7,5},{8,10},{9,11},{10,... | collective-permute-start | bytes 73736 | tf_op jit(solution)/shard_map/ppermute | solution.py:30
  124.1 3.6 %collective-permute-start.2 = (bf16[24,512]{1,0:T(8,128)(2,1)S(1)}, bf16[24,512]{1,0:T(8,128)(2,1)S(1)}, u32[]{:S(2)}, u32[]{:S(2)}) collective-permute-start(bf16[24,512]{1,0:T(8,128)(2,1)S(1)} %get-tuple-element.15.resid), channel_id=1, source_target_pairs={{0,3},{1,0},{2,1},{3,2},{4,7},{5,4},{6,5},{7,6},{8,11},{9,8},{10,9... | collective-permute-start | bytes 73736 | tf_op jit(solution)/shard_map/ppermute | solution.py:30
  127.8 2.7 %expert.1 = bf16[8,4,32,512]{3,2,1,0:T(8,128)(2,1)} custom-call(bf16[8,4,32,512]{3,2,1,0:T(8,128)(2,1)S(1)} %bitcast.68, bf16[1,2048]{1,0:T(2,128)(2,1)S(1)} %broadcast_in_dim.61.gain, bf16[2048,128]{1,0:T(8,128)(2,1)S(1)} %bitcast.76, bf16[2048,128]{1,0:T(8,128)(2,1)S(1)} %bitcast.77, bf16[128,2048]{1,0:T(8,128)(2,1)S(1)} %bitcast.78), custom_call_target="tpu_custom_call" | custom-call | tf_op jit(solution)/shard_map/expert/pallas_call | solution.py:187
  130.5 6.5 %all-to-all-start.5 = ((bf16[32,32,512]{2,1,0:T(8,128)(2,1)}), bf16[32,32,512]{2,1,0:T(8,128)(2,1)S(1)}, u32[]{:S(2)}, u32[]{:S(2)}) async-start(bf16[32,32,512]{2,1,0:T(8,128)(2,1)} %bitcast.24), calls=%async_computation.5 | async-start | bytes 2097152 | tf_op jit(solution)/shard_map/all_to_all | solution.py:19
  137.1 1.2 select_bitcast_fusion.1
  139.5 3.4 %collective-permute-start.4 = (bf16[24,512]{1,0:T(8,128)(2,1)S(1)}, bf16[24,512]{1,0:T(8,128)(2,1)S(1)}, u32[]{:S(2)}, u32[]{:S(2)}) collective-permute-start(bf16[24,512]{1,0:T(8,128)(2,1)S(1)} %get-tuple-element.29), channel_id=1, source_target_pairs={{0,1},{1,2},{2,3},{3,0},{4,5},{5,6},{6,7},{7,4},{8,9},{9,10},{10,1... | collective-permute-start | bytes 73736 | tf_op jit(solution)/shard_map/ppermute | solution.py:30
  142.9 4.6 %collective-permute-start.5 = (bf16[24,512]{1,0:T(8,128)(2,1)S(1)}, bf16[24,512]{1,0:T(8,128)(2,1)S(1)}, u32[]{:S(2)}, u32[]{:S(2)}) collective-permute-start(bf16[24,512]{1,0:T(8,128)(2,1)S(1)} %get-tuple-element.28), channel_id=1, source_target_pairs={{0,2},{1,3},{2,0},{3,1},{4,6},{5,7},{6,4},{7,5},{8,10},{9,11},{10,... | collective-permute-start | bytes 73736 | tf_op jit(solution)/shard_map/ppermute | solution.py:30
  147.5 3.4 %collective-permute-start.6 = (bf16[24,512]{1,0:T(8,128)(2,1)S(1)}, bf16[24,512]{1,0:T(8,128)(2,1)S(1)}, u32[]{:S(2)}, u32[]{:S(2)}) collective-permute-start(bf16[24,512]{1,0:T(8,128)(2,1)S(1)} %get-tuple-element.27), channel_id=1, source_target_pairs={{0,3},{1,0},{2,1},{3,2},{4,7},{5,4},{6,5},{7,6},{8,11},{9,8},{10,9... | collective-permute-start | bytes 73736 | tf_op jit(solution)/shard_map/ppermute | solution.py:30
  150.9 2.5 %collective-permute-done.4.second = bf16[24,512]{1,0:T(8,128)(2,1)S(1)} collective-permute-done((bf16[24,512]{1,0:T(8,128)(2,1)S(1)}, bf16[24,512]{1,0:T(8,128)(2,1)S(1)}, u32[]{:S(2)}, u32[]{:S(2)}) %collective-permute-start.4) | collective-permute-done | bytes 24608 | tf_op jit(solution)/shard_map/ppermute | solution.py:30
  153.8 24.2 %all_to_all.41 = bf16[16,16,512]{2,1,0:T(8,128)(2,1)S(1)} all-to-all(bf16[16,16,512]{2,1,0:T(8,128)(2,1)S(1)} %bitcast.79), channel_id=1, replica_groups=mesh['ep_0'=16,'ep_1'=4,'ep_2'=2,'tp'=4] {'ep_0'}, dimensions={0} | all-to-all | bytes 524288 | tf_op jit(solution)/shard_map/all_to_all | solution.py:19
  178.0 0.9 shard_map.207
  178.9 3.3 %all-to-all-start.7 = ((f32[4,8,128]{2,1,0:T(8,128)}), f32[4,8,128]{2,1,0:T(8,128)S(1)}, u32[]{:S(2)}, u32[]{:S(2)}) async-start(f32[4,8,128]{2,1,0:T(8,128)} %get-tuple-element.20), calls=%async_computation.7 | async-start | bytes 32768 | tf_op jit(solution)/shard_map/all_to_all | solution.py:19
  182.2 5.3 %all-to-all-done.7.squares = f32[4,8,128]{2,1,0:T(8,128)S(1)} async-done(((f32[4,8,128]{2,1,0:T(8,128)}), f32[4,8,128]{2,1,0:T(8,128)S(1)}, u32[]{:S(2)}, u32[]{:S(2)}) %all-to-all-start.7) | async-done | bytes 16416 | tf_op jit(solution)/shard_map/all_to_all | solution.py:19
  (73 shorter events, 6.6 us)
Async XLA Ops:
  0.6 20.9 %copy-start = (bf16[2048,128]{1,0:T(8,128)(2,1)S(1)}, bf16[2048,128]{1,0:T(8,128)(2,1)}, u32[]{:S(2)}) copy-start(bf16[2048,128]{1,0:T(8,128)(2,1)} %param.23) | copy-start | bytes 1572868
  0.6 20.6 %copy-start.7 = (bf16[24,2048]{1,0:T(8,128)(2,1)S(1)}, bf16[24,2048]{1,0:T(8,128)(2,1)}, u32[]{:S(2)}) copy-start(bf16[24,2048]{1,0:T(8,128)(2,1)} %param.20) | copy-start | bytes 294916
  0.7 20.9 %copy-start.15 = (f32[1,128]{1,0:T(1,128)S(1)}, f32[1,128]{1,0:T(1,128)}, u32[]{:S(2)}) copy-start(f32[1,128]{1,0:T(1,128)} %param.25) | copy-start | bytes 1540
  0.7 20.6 %copy-start.9 = (bf16[2048,128]{1,0:T(8,128)(2,1)S(1)}, bf16[2048,128]{1,0:T(8,128)(2,1)}, u32[]{:S(2)}) copy-start(bf16[2048,128]{1,0:T(8,128)(2,1)} %param.22) | copy-start | bytes 1572868
  0.7 21.2 %copy-start.8 = (f32[24,1,128,128]{3,2,1,0:T(8,128)S(1)}, f32[24,1,128,128]{3,2,1,0:T(8,128)}, u32[]{:S(2)}) copy-start(f32[24,1,128,128]{3,2,1,0:T(8,128)} %param.21) | copy-start | bytes 4718596
  2.3 33.6 %all-to-all-start = ((bf16[16,4,16,128]{3,2,1,0:T(8,128)(2,1)}), bf16[16,4,16,128]{3,2,1,0:T(8,128)(2,1)S(1)}, u32[]{:S(2)}, u32[]{:S(2)}) async-start(bf16[16,4,16,128]{3,2,1,0:T(8,128)(2,1)} %broadcast_in_dim.59), calls=%async_computation | async-start | bytes 524288 | tf_op jit(solution)/shard_map/all_to_all | solution.py:19
  22.9 1.9 copy-start.6
  22.9 1.6 copy-start.11
  22.9 1.7 copy-start.12
  22.9 1.8 copy-start.16
  36.5 8.9 %all-to-all-start.1 = ((bf16[8,24,128]{2,1,0:T(8,128)(2,1)}), bf16[8,24,128]{2,1,0:T(8,128)(2,1)S(1)}, u32[]{:S(2)}, u32[]{:S(2)}) async-start(bf16[8,24,128]{2,1,0:T(8,128)(2,1)} %broadcast_in_dim.58), calls=%async_computation.1 | async-start | bytes 98304 | tf_op jit(solution)/shard_map/all_to_all | solution.py:19
  46.3 13.9 %all-to-all-start.2 = ((bf16[32,24,128]{2,1,0:T(8,128)(2,1)}), bf16[32,24,128]{2,1,0:T(8,128)(2,1)S(1)}, u32[]{:S(2)}, u32[]{:S(2)}) async-start(bf16[32,24,128]{2,1,0:T(8,128)(2,1)} %bitcast.14), calls=%async_computation.2 | async-start | bytes 393216 | tf_op jit(solution)/shard_map/all_to_all | solution.py:19
  85.9 41.9 %all-to-all-start.4 = ((bf16[32,32,512]{2,1,0:T(8,128)(2,1)}), bf16[32,32,512]{2,1,0:T(8,128)(2,1)S(1)}, u32[]{:S(2)}, u32[]{:S(2)}) async-start(bf16[32,32,512]{2,1,0:T(8,128)(2,1)} %bitcast.19), calls=%async_computation.4 | async-start | bytes 2097152 | tf_op jit(solution)/shard_map/all_to_all | solution.py:19
  90.8 36.9 %copy-start.10 = (bf16[2048]{0:T(1024)(128)(2,1)S(1)}, bf16[2048]{0:T(1024)(128)(2,1)}, u32[]{:S(2)}) copy-start(bf16[2048]{0:T(1024)(128)(2,1)} %param.29) | copy-start | bytes 12292
  90.8 36.9 %copy-start.13 = (bf16[2048]{0:T(1024)(128)(2,1)S(1)}, bf16[2048]{0:T(1024)(128)(2,1)}, u32[]{:S(2)}) copy-start(bf16[2048]{0:T(1024)(128)(2,1)} %param.31) | copy-start | bytes 12292
  90.9 36.9 %copy-start.1 = (bf16[1,2048,128]{2,1,0:T(8,128)(2,1)S(1)}, bf16[1,2048,128]{2,1,0:T(8,128)(2,1)}, u32[]{:S(2)}) copy-start(bf16[1,2048,128]{2,1,0:T(8,128)(2,1)} %param.37) | copy-start | bytes 1572868
  90.9 36.9 %copy-start.2 = (bf16[1,2048,128]{2,1,0:T(8,128)(2,1)S(1)}, bf16[1,2048,128]{2,1,0:T(8,128)(2,1)}, u32[]{:S(2)}) copy-start(bf16[1,2048,128]{2,1,0:T(8,128)(2,1)} %param.38) | copy-start | bytes 1572868
  90.9 36.9 %copy-start.3 = (bf16[1,128,2048]{2,1,0:T(8,128)(2,1)S(1)}, bf16[1,128,2048]{2,1,0:T(8,128)(2,1)}, u32[]{:S(2)}) copy-start(bf16[1,128,2048]{2,1,0:T(8,128)(2,1)} %param.39) | copy-start | bytes 1572868
  113.4 10.7 %copy-start.4 = (bf16[64,3,16,128]{3,2,1,0:T(8,128)(2,1)}, bf16[64,3,16,128]{3,2,1,0:T(8,128)(2,1)S(1)}, u32[]{:S(2)}) copy-start(bf16[64,3,16,128]{3,2,1,0:T(8,128)(2,1)S(1)} %all-gather) | copy-start | bytes 2359300
  114.5 22.6 %collective-permute-start.3 = (bf16[4,16,3,16,128]{4,3,0,1,2:T(8,128)(2,1)}, bf16[4,16,3,16,128]{4,3,0,1,2:T(8,128)(2,1)}, u32[]{:S(2)}, u32[]{:S(2)}) collective-permute-start(bf16[4,16,3,16,128]{4,3,0,1,2:T(8,128)(2,1)} %copy.38), channel_id=1, source_target_pairs={{0,4},{4,0},{1,5},{5,1},{2,6},{6,2},{3,7},{7,3},{8,12},{12,8},{9,1... | collective-permute-start | bytes 2359304 | tf_op jit(solution)/shard_map/ppermute | solution.py:338
  116.4 20.6 %collective-permute-start = (bf16[24,512]{1,0:T(8,128)(2,1)S(1)}, bf16[24,512]{1,0:T(8,128)(2,1)S(1)}, u32[]{:S(2)}, u32[]{:S(2)}) collective-permute-start(bf16[24,512]{1,0:T(8,128)(2,1)S(1)} %get-tuple-element.15.resid), channel_id=1, source_target_pairs={{0,1},{1,2},{2,3},{3,0},{4,5},{5,6},{6,7},{7,4},{8,9},{9,10},{10,1... | collective-permute-start | bytes 73736 | tf_op jit(solution)/shard_map/ppermute | solution.py:30
  119.7 17.3 %collective-permute-start.1 = (bf16[24,512]{1,0:T(8,128)(2,1)S(1)}, bf16[24,512]{1,0:T(8,128)(2,1)S(1)}, u32[]{:S(2)}, u32[]{:S(2)}) collective-permute-start(bf16[24,512]{1,0:T(8,128)(2,1)S(1)} %get-tuple-element.15.resid), channel_id=1, source_target_pairs={{0,2},{1,3},{2,0},{3,1},{4,6},{5,7},{6,4},{7,5},{8,10},{9,11},{10,... | collective-permute-start | bytes 73736 | tf_op jit(solution)/shard_map/ppermute | solution.py:30
  124.1 13.0 %collective-permute-start.2 = (bf16[24,512]{1,0:T(8,128)(2,1)S(1)}, bf16[24,512]{1,0:T(8,128)(2,1)S(1)}, u32[]{:S(2)}, u32[]{:S(2)}) collective-permute-start(bf16[24,512]{1,0:T(8,128)(2,1)S(1)} %get-tuple-element.15.resid), channel_id=1, source_target_pairs={{0,3},{1,0},{2,1},{3,2},{4,7},{5,4},{6,5},{7,6},{8,11},{9,8},{10,9... | collective-permute-start | bytes 73736 | tf_op jit(solution)/shard_map/ppermute | solution.py:30
  130.5 6.6 %copy-start.5 = (bf16[64,3,16,128]{3,2,1,0:T(8,128)(2,1)S(1)}, bf16[64,3,16,128]{3,2,1,0:T(8,128)(2,1)}, u32[]{:S(2)}) copy-start(bf16[64,3,16,128]{3,2,1,0:T(8,128)(2,1)} %copy-done.4) | copy-start | bytes 2359300
  130.5 22.9 %all-to-all-start.5 = ((bf16[32,32,512]{2,1,0:T(8,128)(2,1)}), bf16[32,32,512]{2,1,0:T(8,128)(2,1)S(1)}, u32[]{:S(2)}, u32[]{:S(2)}) async-start(bf16[32,32,512]{2,1,0:T(8,128)(2,1)} %bitcast.24), calls=%async_computation.5 | async-start | bytes 2097152 | tf_op jit(solution)/shard_map/all_to_all | solution.py:19
  138.9 43.3 %copy-start.14 = (bf16[512]{0:T(512)(128)(2,1)S(1)}, bf16[512]{0:T(512)(128)(2,1)}, u32[]{:S(2)}) copy-start(bf16[512]{0:T(512)(128)(2,1)} %param.30) | copy-start | bytes 3076
  139.5 13.9 %collective-permute-start.4 = (bf16[24,512]{1,0:T(8,128)(2,1)S(1)}, bf16[24,512]{1,0:T(8,128)(2,1)S(1)}, u32[]{:S(2)}, u32[]{:S(2)}) collective-permute-start(bf16[24,512]{1,0:T(8,128)(2,1)S(1)} %get-tuple-element.29), channel_id=1, source_target_pairs={{0,1},{1,2},{2,3},{3,0},{4,5},{5,6},{6,7},{7,4},{8,9},{9,10},{10,1... | collective-permute-start | bytes 73736 | tf_op jit(solution)/shard_map/ppermute | solution.py:30
  142.9 10.5 %collective-permute-start.5 = (bf16[24,512]{1,0:T(8,128)(2,1)S(1)}, bf16[24,512]{1,0:T(8,128)(2,1)S(1)}, u32[]{:S(2)}, u32[]{:S(2)}) collective-permute-start(bf16[24,512]{1,0:T(8,128)(2,1)S(1)} %get-tuple-element.28), channel_id=1, source_target_pairs={{0,2},{1,3},{2,0},{3,1},{4,6},{5,7},{6,4},{7,5},{8,10},{9,11},{10,... | collective-permute-start | bytes 73736 | tf_op jit(solution)/shard_map/ppermute | solution.py:30
  147.5 5.9 %collective-permute-start.6 = (bf16[24,512]{1,0:T(8,128)(2,1)S(1)}, bf16[24,512]{1,0:T(8,128)(2,1)S(1)}, u32[]{:S(2)}, u32[]{:S(2)}) collective-permute-start(bf16[24,512]{1,0:T(8,128)(2,1)S(1)} %get-tuple-element.27), channel_id=1, source_target_pairs={{0,3},{1,0},{2,1},{3,2},{4,7},{5,4},{6,5},{7,6},{8,11},{9,8},{10,9... | collective-permute-start | bytes 73736 | tf_op jit(solution)/shard_map/ppermute | solution.py:30
  178.9 8.6 %all-to-all-start.7 = ((f32[4,8,128]{2,1,0:T(8,128)}), f32[4,8,128]{2,1,0:T(8,128)S(1)}, u32[]{:S(2)}, u32[]{:S(2)}) async-start(f32[4,8,128]{2,1,0:T(8,128)} %get-tuple-element.20), calls=%async_computation.7 | async-start | bytes 32768 | tf_op jit(solution)/shard_map/all_to_all | solution.py:19

commit v5 on v4

--- a/solution.py
+++ b/solution.py
@@ -39,8 +39,10 @@
     n = cores * zs * 2
     core_major = lax.broadcasted_iota(jnp.int32, (n, n), 1 if inverse else 0)
     z_major = lax.broadcasted_iota(jnp.int32, (n, n), 0 if inverse else 1)
-    core, z, slot = core_major // (2 * zs), (core_major // 2) % zs, core_major % 2
-    return jnp.where(z_major == (z * cores + core) * 2 + slot, 1.0, 0.0).astype(BF)
+    core = core_major >> (2 * zs).bit_length() - 1
+    z = (core_major >> 1) & (zs - 1)
+    place = (((z << cores.bit_length() - 1) | core) << 1) | (core_major & 1)
+    return jnp.where(z_major == place, 1.0, 0.0).astype(BF)
 
 
 def vmem_call(body, out_shape, args, scratch=(), limit=32):

time: 189 us -> 189 us (level)
  no operation moved by 1% of the time
where the time goes in v5:
time: 189 us; the launch traced here: 188 us
  blocking collectives  70.7 us (37%)
  starting transfers between devices  66 us (35%)
  waiting for transfers between devices  29.9 us (16%)
  Pallas kernels  7.65 us (4%)
  other arithmetic  6.1 us (3%)
  matrix products  3.4 us (2%)
  local copies, waits for them, and re-layouts  3.2 us (2%)
    all_to_all x2, blocking collectives, exchanged(): return lax.all_to_all(value, axes, 0, 0, tiled=True)  48.3 us
    all_to_all x6, starting transfers between devices, exchanged(): return lax.all_to_all(value, axes, 0, 0, tiled=True)  41.5 us
    all_to_all x6, waiting for transfers between devices, exchanged(): return lax.all_to_all(value, axes, 0, 0, tiled=True)  27.4 us
    ppermute x6, starting transfers between devices, turned(): lax.ppermute(value, 'tp', [(k, (k + step) % devices) for k in range(devic...  22.6 us
    all_gather x1, blocking collectives, shards(): shared = lax.all_gather(parts[:, 1:], 'ep_1')  22.4 us
    pallas_call x6, Pallas kernels, vmem_call(): pl.pallas_call(body, out_shape=out_shape, in_specs=[vmem] * len(args), ou...  4.39 us
  transfers between devices with their start and end apart: 13, of which 5 were waited for; matrix products, arithmetic and copies ran while one was open for 5% of the time, Pallas kernels for 2%

profile of v5, /device:TPU:2, one launch (start us, length us, event | category | flops | bytes accessed | tf_op | source)
XLA Modules:
  0.0 188.2 jit_solution(10086278983468438423)
XLA Ops:
  0.7 0.9 pad_maximum_fusion.1
  2.3 15.2 %all-to-all-start = ((bf16[16,4,16,128]{3,2,1,0:T(8,128)(2,1)}), bf16[16,4,16,128]{3,2,1,0:T(8,128)(2,1)S(1)}, u32[]{:S(2)}, u32[]{:S(2)}) async-start(bf16[16,4,16,128]{3,2,1,0:T(8,128)(2,1)} %broadcast_in_dim.59), calls=%async_computation | async-start | bytes 524288 | tf_op jit(solution)/shard_map/all_to_all | solution.py:19
  18.2 1.0 fusion.3
  19.9 1.3 fusion.11
  21.8 1.0 multiply_add_fusion
  22.9 1.4 fusion
  24.8 11.1 %all-to-all-done.parts = bf16[16,4,16,128]{3,2,1,0:T(8,128)(2,1)S(1)} async-done(((bf16[16,4,16,128]{3,2,1,0:T(8,128)(2,1)}), bf16[16,4,16,128]{3,2,1,0:T(8,128)(2,1)S(1)}, u32[]{:S(2)}, u32[]{:S(2)}) %all-to-all-start) | async-done | bytes 262176 | tf_op jit(solution)/shard_map/all_to_all | solution.py:19
  36.5 4.8 %all-to-all-start.1 = ((bf16[8,24,128]{2,1,0:T(8,128)(2,1)}), bf16[8,24,128]{2,1,0:T(8,128)(2,1)S(1)}, u32[]{:S(2)}, u32[]{:S(2)}) async-start(bf16[8,24,128]{2,1,0:T(8,128)(2,1)} %broadcast_in_dim.58), calls=%async_computation.1 | async-start | bytes 98304 | tf_op jit(solution)/shard_map/all_to_all | solution.py:19
  41.4 4.1 %all-to-all-done.1.heads = bf16[8,24,128]{2,1,0:T(8,128)(2,1)S(1)} async-done(((bf16[8,24,128]{2,1,0:T(8,128)(2,1)}), bf16[8,24,128]{2,1,0:T(8,128)(2,1)S(1)}, u32[]{:S(2)}, u32[]{:S(2)}) %all-to-all-start.1) | async-done | bytes 49184 | tf_op jit(solution)/shard_map/all_to_all | solution.py:19
  45.4 0.9 shard_map.203
  46.3 6.7 %all-to-all-start.2 = ((bf16[32,24,128]{2,1,0:T(8,128)(2,1)}), bf16[32,24,128]{2,1,0:T(8,128)(2,1)S(1)}, u32[]{:S(2)}, u32[]{:S(2)}) async-start(bf16[32,24,128]{2,1,0:T(8,128)(2,1)} %bitcast.14), calls=%async_computation.2 | async-start | bytes 393216 | tf_op jit(solution)/shard_map/all_to_all | solution.py:19
  53.3 7.0 %all-to-all-done.2 = bf16[32,24,128]{2,1,0:T(8,128)(2,1)S(1)} async-done(((bf16[32,24,128]{2,1,0:T(8,128)(2,1)}), bf16[32,24,128]{2,1,0:T(8,128)(2,1)S(1)}, u32[]{:S(2)}, u32[]{:S(2)}) %all-to-all-start.2) | async-done | bytes 196640 | tf_op jit(solution)/shard_map/all_to_all | solution.py:19
  60.6 24.0 %all_to_all.40 = bf16[16,16,512]{2,1,0:T(8,128)(2,1)S(1)} all-to-all(bf16[16,16,512]{2,1,0:T(8,128)(2,1)S(1)} %bitcast.80), channel_id=1, replica_groups=mesh['ep_0'=16,'ep_1'=4,'ep_2'=2,'tp'=4] {'ep_0'}, dimensions={0} | all-to-all | bytes 524288 | tf_op jit(solution)/shard_map/all_to_all | solution.py:19
  84.6 1.2 shard_map.205
  85.9 5.0 %all-to-all-start.4 = ((bf16[32,32,512]{2,1,0:T(8,128)(2,1)}), bf16[32,32,512]{2,1,0:T(8,128)(2,1)S(1)}, u32[]{:S(2)}, u32[]{:S(2)}) async-start(bf16[32,32,512]{2,1,0:T(8,128)(2,1)} %bitcast.19), calls=%async_computation.4 | async-start | bytes 2097152 | tf_op jit(solution)/shard_map/all_to_all | solution.py:19
  90.9 22.4 %all-gather = bf16[64,3,16,128]{3,2,1,0:T(8,128)(2,1)S(1)} all-gather(bf16[16,3,16,128]{3,2,1,0:T(8,128)(2,1)S(1)} %slice.27), channel_id=2, replica_groups=mesh['ep_0'=16,'ep_1'=4,'ep_2'=2,'tp'=4] {'ep_1'}, dimensions={0}, use_global_device_ids=true | all-gather | bytes 983040 | tf_op jit(solution)/shard_map/all_gather | solution.py:339
  113.4 1.1 copy.38
  114.5 1.9 %collective-permute-start.3 = (bf16[4,16,3,16,128]{4,3,0,1,2:T(8,128)(2,1)}, bf16[4,16,3,16,128]{4,3,0,1,2:T(8,128)(2,1)}, u32[]{:S(2)}, u32[]{:S(2)}) collective-permute-start(bf16[4,16,3,16,128]{4,3,0,1,2:T(8,128)(2,1)} %copy.38), channel_id=1, source_target_pairs={{0,4},{4,0},{1,5},{5,1},{2,6},{6,2},{3,7},{7,3},{8,12},{12,8},{9,1... | collective-permute-start | bytes 2359304 | tf_op jit(solution)/shard_map/ppermute | solution.py:340
  116.4 3.3 %collective-permute-start = (bf16[24,512]{1,0:T(8,128)(2,1)S(1)}, bf16[24,512]{1,0:T(8,128)(2,1)S(1)}, u32[]{:S(2)}, u32[]{:S(2)}) collective-permute-start(bf16[24,512]{1,0:T(8,128)(2,1)S(1)} %get-tuple-element.15.resid), channel_id=1, source_target_pairs={{0,1},{1,2},{2,3},{3,0},{4,5},{5,6},{6,7},{7,4},{8,9},{9,10},{10,1... | collective-permute-start | bytes 73736 | tf_op jit(solution)/shard_map/ppermute | solution.py:30
  119.7 4.4 %collective-permute-start.1 = (bf16[24,512]{1,0:T(8,128)(2,1)S(1)}, bf16[24,512]{1,0:T(8,128)(2,1)S(1)}, u32[]{:S(2)}, u32[]{:S(2)}) collective-permute-start(bf16[24,512]{1,0:T(8,128)(2,1)S(1)} %get-tuple-element.15.resid), channel_id=1, source_target_pairs={{0,2},{1,3},{2,0},{3,1},{4,6},{5,7},{6,4},{7,5},{8,10},{9,11},{10,... | collective-permute-start | bytes 73736 | tf_op jit(solution)/shard_map/ppermute | solution.py:30
  124.1 3.6 %collective-permute-start.2 = (bf16[24,512]{1,0:T(8,128)(2,1)S(1)}, bf16[24,512]{1,0:T(8,128)(2,1)S(1)}, u32[]{:S(2)}, u32[]{:S(2)}) collective-permute-start(bf16[24,512]{1,0:T(8,128)(2,1)S(1)} %get-tuple-element.15.resid), channel_id=1, source_target_pairs={{0,3},{1,0},{2,1},{3,2},{4,7},{5,4},{6,5},{7,6},{8,11},{9,8},{10,9... | collective-permute-start | bytes 73736 | tf_op jit(solution)/shard_map/ppermute | solution.py:30
  127.8 2.7 %expert.1 = bf16[8,4,32,512]{3,2,1,0:T(8,128)(2,1)} custom-call(bf16[8,4,32,512]{3,2,1,0:T(8,128)(2,1)S(1)} %bitcast.68, bf16[1,2048]{1,0:T(2,128)(2,1)S(1)} %broadcast_in_dim.61.gain, bf16[2048,128]{1,0:T(8,128)(2,1)S(1)} %bitcast.76, bf16[2048,128]{1,0:T(8,128)(2,1)S(1)} %bitcast.77, bf16[128,2048]{1,0:T(8,128)(2,1)S(1)} %bitcast.78), custom_call_target="tpu_custom_call" | custom-call | tf_op jit(solution)/shard_map/expert/pallas_call | solution.py:189
  130.5 6.5 %all-to-all-start.5 = ((bf16[32,32,512]{2,1,0:T(8,128)(2,1)}), bf16[32,32,512]{2,1,0:T(8,128)(2,1)S(1)}, u32[]{:S(2)}, u32[]{:S(2)}) async-start(bf16[32,32,512]{2,1,0:T(8,128)(2,1)} %bitcast.24), calls=%async_computation.5 | async-start | bytes 2097152 | tf_op jit(solution)/shard_map/all_to_all | solution.py:19
  137.1 1.2 select_bitcast_fusion.1
  139.5 3.4 %collective-permute-start.4 = (bf16[24,512]{1,0:T(8,128)(2,1)S(1)}, bf16[24,512]{1,0:T(8,128)(2,1)S(1)}, u32[]{:S(2)}, u32[]{:S(2)}) collective-permute-start(bf16[24,512]{1,0:T(8,128)(2,1)S(1)} %get-tuple-element.29), channel_id=1, source_target_pairs={{0,1},{1,2},{2,3},{3,0},{4,5},{5,6},{6,7},{7,4},{8,9},{9,10},{10,1... | collective-permute-start | bytes 73736 | tf_op jit(solution)/shard_map/ppermute | solution.py:30
  142.9 4.6 %collective-permute-start.5 = (bf16[24,512]{1,0:T(8,128)(2,1)S(1)}, bf16[24,512]{1,0:T(8,128)(2,1)S(1)}, u32[]{:S(2)}, u32[]{:S(2)}) collective-permute-start(bf16[24,512]{1,0:T(8,128)(2,1)S(1)} %get-tuple-element.28), channel_id=1, source_target_pairs={{0,2},{1,3},{2,0},{3,1},{4,6},{5,7},{6,4},{7,5},{8,10},{9,11},{10,... | collective-permute-start | bytes 73736 | tf_op jit(solution)/shard_map/ppermute | solution.py:30
  147.5 3.4 %collective-permute-start.6 = (bf16[24,512]{1,0:T(8,128)(2,1)S(1)}, bf16[24,512]{1,0:T(8,128)(2,1)S(1)}, u32[]{:S(2)}, u32[]{:S(2)}) collective-permute-start(bf16[24,512]{1,0:T(8,128)(2,1)S(1)} %get-tuple-element.27), channel_id=1, source_target_pairs={{0,3},{1,0},{2,1},{3,2},{4,7},{5,4},{6,5},{7,6},{8,11},{9,8},{10,9... | collective-permute-start | bytes 73736 | tf_op jit(solution)/shard_map/ppermute | solution.py:30
  150.9 2.5 %collective-permute-done.4.second = bf16[24,512]{1,0:T(8,128)(2,1)S(1)} collective-permute-done((bf16[24,512]{1,0:T(8,128)(2,1)S(1)}, bf16[24,512]{1,0:T(8,128)(2,1)S(1)}, u32[]{:S(2)}, u32[]{:S(2)}) %collective-permute-start.4) | collective-permute-done | bytes 24608 | tf_op jit(solution)/shard_map/ppermute | solution.py:30
  153.8 24.2 %all_to_all.41 = bf16[16,16,512]{2,1,0:T(8,128)(2,1)S(1)} all-to-all(bf16[16,16,512]{2,1,0:T(8,128)(2,1)S(1)} %bitcast.79), channel_id=1, replica_groups=mesh['ep_0'=16,'ep_1'=4,'ep_2'=2,'tp'=4] {'ep_0'}, dimensions={0} | all-to-all | bytes 524288 | tf_op jit(solution)/shard_map/all_to_all | solution.py:19
  178.0 0.9 shard_map.207
  178.9 3.3 %all-to-all-start.7 = ((f32[4,8,128]{2,1,0:T(8,128)}), f32[4,8,128]{2,1,0:T(8,128)S(1)}, u32[]{:S(2)}, u32[]{:S(2)}) async-start(f32[4,8,128]{2,1,0:T(8,128)} %get-tuple-element.20), calls=%async_computation.7 | async-start | bytes 32768 | tf_op jit(solution)/shard_map/all_to_all | solution.py:19
  182.2 5.3 %all-to-all-done.7.squares = f32[4,8,128]{2,1,0:T(8,128)S(1)} async-done(((f32[4,8,128]{2,1,0:T(8,128)}), f32[4,8,128]{2,1,0:T(8,128)S(1)}, u32[]{:S(2)}, u32[]{:S(2)}) %all-to-all-start.7) | async-done | bytes 16416 | tf_op jit(solution)/shard_map/all_to_all | solution.py:19
  (73 shorter events, 6.6 us)
Async XLA Ops:
  0.6 20.9 %copy-start = (bf16[2048,128]{1,0:T(8,128)(2,1)S(1)}, bf16[2048,128]{1,0:T(8,128)(2,1)}, u32[]{:S(2)}) copy-start(bf16[2048,128]{1,0:T(8,128)(2,1)} %param.23) | copy-start | bytes 1572868
  0.6 20.6 %copy-start.7 = (bf16[24,2048]{1,0:T(8,128)(2,1)S(1)}, bf16[24,2048]{1,0:T(8,128)(2,1)}, u32[]{:S(2)}) copy-start(bf16[24,2048]{1,0:T(8,128)(2,1)} %param.20) | copy-start | bytes 294916
  0.7 20.9 %copy-start.15 = (f32[1,128]{1,0:T(1,128)S(1)}, f32[1,128]{1,0:T(1,128)}, u32[]{:S(2)}) copy-start(f32[1,128]{1,0:T(1,128)} %param.25) | copy-start | bytes 1540
  0.7 20.6 %copy-start.9 = (bf16[2048,128]{1,0:T(8,128)(2,1)S(1)}, bf16[2048,128]{1,0:T(8,128)(2,1)}, u32[]{:S(2)}) copy-start(bf16[2048,128]{1,0:T(8,128)(2,1)} %param.22) | copy-start | bytes 1572868
  0.7 21.2 %copy-start.8 = (f32[24,1,128,128]{3,2,1,0:T(8,128)S(1)}, f32[24,1,128,128]{3,2,1,0:T(8,128)}, u32[]{:S(2)}) copy-start(f32[24,1,128,128]{3,2,1,0:T(8,128)} %param.21) | copy-start | bytes 4718596
  2.3 33.6 %all-to-all-start = ((bf16[16,4,16,128]{3,2,1,0:T(8,128)(2,1)}), bf16[16,4,16,128]{3,2,1,0:T(8,128)(2,1)S(1)}, u32[]{:S(2)}, u32[]{:S(2)}) async-start(bf16[16,4,16,128]{3,2,1,0:T(8,128)(2,1)} %broadcast_in_dim.59), calls=%async_computation | async-start | bytes 524288 | tf_op jit(solution)/shard_map/all_to_all | solution.py:19
  22.9 1.9 copy-start.6
  22.9 1.6 copy-start.11
  22.9 1.7 copy-start.12
  22.9 1.8 copy-start.16
  36.5 8.9 %all-to-all-start.1 = ((bf16[8,24,128]{2,1,0:T(8,128)(2,1)}), bf16[8,24,128]{2,1,0:T(8,128)(2,1)S(1)}, u32[]{:S(2)}, u32[]{:S(2)}) async-start(bf16[8,24,128]{2,1,0:T(8,128)(2,1)} %broadcast_in_dim.58), calls=%async_computation.1 | async-start | bytes 98304 | tf_op jit(solution)/shard_map/all_to_all | solution.py:19
  46.3 13.9 %all-to-all-start.2 = ((bf16[32,24,128]{2,1,0:T(8,128)(2,1)}), bf16[32,24,128]{2,1,0:T(8,128)(2,1)S(1)}, u32[]{:S(2)}, u32[]{:S(2)}) async-start(bf16[32,24,128]{2,1,0:T(8,128)(2,1)} %bitcast.14), calls=%async_computation.2 | async-start | bytes 393216 | tf_op jit(solution)/shard_map/all_to_all | solution.py:19
  85.9 41.9 %all-to-all-start.4 = ((bf16[32,32,512]{2,1,0:T(8,128)(2,1)}), bf16[32,32,512]{2,1,0:T(8,128)(2,1)S(1)}, u32[]{:S(2)}, u32[]{:S(2)}) async-start(bf16[32,32,512]{2,1,0:T(8,128)(2,1)} %bitcast.19), calls=%async_computation.4 | async-start | bytes 2097152 | tf_op jit(solution)/shard_map/all_to_all | solution.py:19
  90.8 36.9 %copy-start.10 = (bf16[2048]{0:T(1024)(128)(2,1)S(1)}, bf16[2048]{0:T(1024)(128)(2,1)}, u32[]{:S(2)}) copy-start(bf16[2048]{0:T(1024)(128)(2,1)} %param.29) | copy-start | bytes 12292
  90.8 36.9 %copy-start.13 = (bf16[2048]{0:T(1024)(128)(2,1)S(1)}, bf16[2048]{0:T(1024)(128)(2,1)}, u32[]{:S(2)}) copy-start(bf16[2048]{0:T(1024)(128)(2,1)} %param.31) | copy-start | bytes 12292
  90.9 36.9 %copy-start.1 = (bf16[1,2048,128]{2,1,0:T(8,128)(2,1)S(1)}, bf16[1,2048,128]{2,1,0:T(8,128)(2,1)}, u32[]{:S(2)}) copy-start(bf16[1,2048,128]{2,1,0:T(8,128)(2,1)} %param.37) | copy-start | bytes 1572868
  90.9 36.9 %copy-start.2 = (bf16[1,2048,128]{2,1,0:T(8,128)(2,1)S(1)}, bf16[1,2048,128]{2,1,0:T(8,128)(2,1)}, u32[]{:S(2)}) copy-start(bf16[1,2048,128]{2,1,0:T(8,128)(2,1)} %param.38) | copy-start | bytes 1572868
  90.9 36.9 %copy-start.3 = (bf16[1,128,2048]{2,1,0:T(8,128)(2,1)S(1)}, bf16[1,128,2048]{2,1,0:T(8,128)(2,1)}, u32[]{:S(2)}) copy-start(bf16[1,128,2048]{2,1,0:T(8,128)(2,1)} %param.39) | copy-start | bytes 1572868
  113.4 10.7 %copy-start.4 = (bf16[64,3,16,128]{3,2,1,0:T(8,128)(2,1)}, bf16[64,3,16,128]{3,2,1,0:T(8,128)(2,1)S(1)}, u32[]{:S(2)}) copy-start(bf16[64,3,16,128]{3,2,1,0:T(8,128)(2,1)S(1)} %all-gather) | copy-start | bytes 2359300
  114.5 22.6 %collective-permute-start.3 = (bf16[4,16,3,16,128]{4,3,0,1,2:T(8,128)(2,1)}, bf16[4,16,3,16,128]{4,3,0,1,2:T(8,128)(2,1)}, u32[]{:S(2)}, u32[]{:S(2)}) collective-permute-start(bf16[4,16,3,16,128]{4,3,0,1,2:T(8,128)(2,1)} %copy.38), channel_id=1, source_target_pairs={{0,4},{4,0},{1,5},{5,1},{2,6},{6,2},{3,7},{7,3},{8,12},{12,8},{9,1... | collective-permute-start | bytes 2359304 | tf_op jit(solution)/shard_map/ppermute | solution.py:340
  116.4 20.6 %collective-permute-start = (bf16[24,512]{1,0:T(8,128)(2,1)S(1)}, bf16[24,512]{1,0:T(8,128)(2,1)S(1)}, u32[]{:S(2)}, u32[]{:S(2)}) collective-permute-start(bf16[24,512]{1,0:T(8,128)(2,1)S(1)} %get-tuple-element.15.resid), channel_id=1, source_target_pairs={{0,1},{1,2},{2,3},{3,0},{4,5},{5,6},{6,7},{7,4},{8,9},{9,10},{10,1... | collective-permute-start | bytes 73736 | tf_op jit(solution)/shard_map/ppermute | solution.py:30
  119.7 17.3 %collective-permute-start.1 = (bf16[24,512]{1,0:T(8,128)(2,1)S(1)}, bf16[24,512]{1,0:T(8,128)(2,1)S(1)}, u32[]{:S(2)}, u32[]{:S(2)}) collective-permute-start(bf16[24,512]{1,0:T(8,128)(2,1)S(1)} %get-tuple-element.15.resid), channel_id=1, source_target_pairs={{0,2},{1,3},{2,0},{3,1},{4,6},{5,7},{6,4},{7,5},{8,10},{9,11},{10,... | collective-permute-start | bytes 73736 | tf_op jit(solution)/shard_map/ppermute | solution.py:30
  124.1 13.0 %collective-permute-start.2 = (bf16[24,512]{1,0:T(8,128)(2,1)S(1)}, bf16[24,512]{1,0:T(8,128)(2,1)S(1)}, u32[]{:S(2)}, u32[]{:S(2)}) collective-permute-start(bf16[24,512]{1,0:T(8,128)(2,1)S(1)} %get-tuple-element.15.resid), channel_id=1, source_target_pairs={{0,3},{1,0},{2,1},{3,2},{4,7},{5,4},{6,5},{7,6},{8,11},{9,8},{10,9... | collective-permute-start | bytes 73736 | tf_op jit(solution)/shard_map/ppermute | solution.py:30
  130.5 6.6 %copy-start.5 = (bf16[64,3,16,128]{3,2,1,0:T(8,128)(2,1)S(1)}, bf16[64,3,16,128]{3,2,1,0:T(8,128)(2,1)}, u32[]{:S(2)}) copy-start(bf16[64,3,16,128]{3,2,1,0:T(8,128)(2,1)} %copy-done.4) | copy-start | bytes 2359300
  130.5 22.9 %all-to-all-start.5 = ((bf16[32,32,512]{2,1,0:T(8,128)(2,1)}), bf16[32,32,512]{2,1,0:T(8,128)(2,1)S(1)}, u32[]{:S(2)}, u32[]{:S(2)}) async-start(bf16[32,32,512]{2,1,0:T(8,128)(2,1)} %bitcast.24), calls=%async_computation.5 | async-start | bytes 2097152 | tf_op jit(solution)/shard_map/all_to_all | solution.py:19
  138.9 43.3 %copy-start.14 = (bf16[512]{0:T(512)(128)(2,1)S(1)}, bf16[512]{0:T(512)(128)(2,1)}, u32[]{:S(2)}) copy-start(bf16[512]{0:T(512)(128)(2,1)} %param.30) | copy-start | bytes 3076
  139.5 13.9 %collective-permute-start.4 = (bf16[24,512]{1,0:T(8,128)(2,1)S(1)}, bf16[24,512]{1,0:T(8,128)(2,1)S(1)}, u32[]{:S(2)}, u32[]{:S(2)}) collective-permute-start(bf16[24,512]{1,0:T(8,128)(2,1)S(1)} %get-tuple-element.29), channel_id=1, source_target_pairs={{0,1},{1,2},{2,3},{3,0},{4,5},{5,6},{6,7},{7,4},{8,9},{9,10},{10,1... | collective-permute-start | bytes 73736 | tf_op jit(solution)/shard_map/ppermute | solution.py:30
  142.9 10.5 %collective-permute-start.5 = (bf16[24,512]{1,0:T(8,128)(2,1)S(1)}, bf16[24,512]{1,0:T(8,128)(2,1)S(1)}, u32[]{:S(2)}, u32[]{:S(2)}) collective-permute-start(bf16[24,512]{1,0:T(8,128)(2,1)S(1)} %get-tuple-element.28), channel_id=1, source_target_pairs={{0,2},{1,3},{2,0},{3,1},{4,6},{5,7},{6,4},{7,5},{8,10},{9,11},{10,... | collective-permute-start | bytes 73736 | tf_op jit(solution)/shard_map/ppermute | solution.py:30
  147.5 5.9 %collective-permute-start.6 = (bf16[24,512]{1,0:T(8,128)(2,1)S(1)}, bf16[24,512]{1,0:T(8,128)(2,1)S(1)}, u32[]{:S(2)}, u32[]{:S(2)}) collective-permute-start(bf16[24,512]{1,0:T(8,128)(2,1)S(1)} %get-tuple-element.27), channel_id=1, source_target_pairs={{0,3},{1,0},{2,1},{3,2},{4,7},{5,4},{6,5},{7,6},{8,11},{9,8},{10,9... | collective-permute-start | bytes 73736 | tf_op jit(solution)/shard_map/ppermute | solution.py:30
  178.9 8.6 %all-to-all-start.7 = ((f32[4,8,128]{2,1,0:T(8,128)}), f32[4,8,128]{2,1,0:T(8,128)S(1)}, u32[]{:S(2)}, u32[]{:S(2)}) async-start(f32[4,8,128]{2,1,0:T(8,128)} %get-tuple-element.20), calls=%async_computation.7 | async-start | bytes 32768 | tf_op jit(solution)/shard_map/all_to_all | solution.py:19
